TPU v7x, 256 devices: a whole 4x4x8 slice. The times are simulated.
256 devices in a mesh: kv: 16 (over y, x), tp: 16 (over z, core).
Axes of the slice: x: 4, y: 4, z: 8, core: 2. Of those that a mesh axis runs over, the one named last changes fastest.
Arguments:
- tokens: bfloat16 [128, 4096], P(None, ('kv', 'tp')), may hold values from -41 to 41
- lengths: int32 [128], P('kv'), may hold values from 1 to 8192, 262144 in all
- retention_state: float32 [128, 16, 128, 256], P('kv', 'tp'), may hold values from -4 to 4
- mixer_gain: float32 [4096], P('kv'), may hold values from 0.1 to 1.9
- query_weight: bfloat16 [4096, 2048], P('kv', 'tp'), may hold values from -0.09375 to 0.09375
- key_weight: bfloat16 [4096, 2048], P('kv', 'tp'), may hold values from -0.09375 to 0.09375
- value_weight: bfloat16 [4096, 4096], P('kv', 'tp'), may hold values from -0.09375 to 0.09375
- gate_weight: bfloat16 [4096, 4096], P('kv', 'tp'), may hold values from -0.09375 to 0.09375
- output_weight: bfloat16 [4096, 4096], P('tp', 'kv'), may hold values from -0.125 to 0.125
- channel_gain: float32 [4096], P('kv'), may hold values from 0.1 to 1.9
- ffn_gate: bfloat16 [4096, 11264], P('kv', 'tp'), may hold values from -0.09375 to 0.09375
- ffn_up: bfloat16 [4096, 11264], P('kv', 'tp'), may hold values from -0.09375 to 0.09375
- ffn_down: bfloat16 [11264, 4096], P('tp', 'kv'), may hold values from -0.078125 to 0.078125
Outputs:
- layer_output: bfloat16 [128, 4096], P(None, ('kv', 'tp'))
- new_state: float32 [128, 16, 128, 256], P('kv', 'tp')
All inputs are finite; a program needn't handle non-finite values. No bound on the sum of `lengths` on one device may be relied on, other than what follows from the above.
Results may differ from a plain program's by a relative error of at most 0.022.
Values may be sent and summed in bfloat16 or wider, within the bound.
No kernel may reach another device: no remote copies, remote signals or barrier semaphores. Data moves between devices by JAX's collectives and lax.ppermute only.
A program may use at most 64 MiB of HBM per device.

v0:
```python
import jax
import jax.numpy as jnp
from jax import lax
from jax.sharding import PartitionSpec as P

D = 4096
HEADS = 16
QK = 128


def in_blocks(value, dim, devices):
    lengths = value.shape
    blocks = value.reshape(*lengths[:dim], devices, lengths[dim] // devices, *lengths[dim + 1 :])
    return jnp.moveaxis(blocks, dim, 0)


def sent_and_summed(value, axis, dim):
    blocks = in_blocks(value, dim, lax.axis_size(axis))
    arrived = lax.all_to_all(blocks, axis, split_axis=0, concat_axis=0, tiled=True)
    return arrived.astype(jnp.float32).sum(axis=0)


def in_one_piece(arrays, axis, dim, along):
    columns = [a.reshape(*a.shape[:along], -1) for a in arrays]
    both = jnp.concatenate(columns, axis=along)
    result, at, finished = (sent_and_summed(both, axis, dim), 0, [])
    for a, column in zip(arrays, columns):
        piece = result[..., at : at + column.shape[along]]
        finished.append(piece.reshape(*piece.shape[:along], *a.shape[along:]))
        at += column.shape[along]
    return tuple(finished)


def copy_for_each(value, axis):
    devices = lax.axis_size(axis)
    return lax.all_to_all(
        jnp.broadcast_to(value[None], (devices, *value.shape)), axis, 0, 0, tiled=True
    )


def joined_along(blocks, dim):
    blocks = jnp.moveaxis(blocks, 0, dim)
    lengths = blocks.shape
    return blocks.reshape(*lengths[:dim], lengths[dim] * lengths[dim + 1], *lengths[dim + 2 :])


def gather_directly(value, axis, dim):
    blocks = copy_for_each(value, axis)
    return joined_along(blocks, dim)


def rotate_heads(vectors, positions):
    half_dim = vectors.shape[-1] // 2
    frequency = 10000.0 ** (-jnp.arange(half_dim, dtype=jnp.float32) / half_dim)
    angles = positions.astype(jnp.float32)[:, None, None] * frequency
    cosine = jnp.cos(angles)
    sine_part = jnp.sin(angles)
    first_half = vectors[..., :half_dim]
    second = vectors[..., half_dim:]
    return jnp.concatenate(
        [first_half * cosine - second * sine_part, first_half * sine_part + second * cosine],
        axis=-1,
    )


def gathered_rows(columns):
    return lax.all_gather(columns, "tp", axis=1, tiled=True)


def owned_sums(partial_value, squares):
    raw_sums, totals = in_one_piece(
        (partial_value.astype(jnp.bfloat16), squares.astype(jnp.bfloat16)), "kv", 0, 1
    )
    summed = raw_sums * lax.rsqrt(totals / D + 1e-06)[:, None]
    return summed


def on_device(
    tokens,
    lengths,
    retention_state,
    mixer_gain,
    query_weight,
    key_weight,
    value_weight,
    gate_weight,
    output_weight,
    channel_gain,
    ffn_gate,
    ffn_up,
    ffn_down,
):
    feature_block = gathered_rows(tokens).astype(jnp.float32)
    squares = jnp.sum(feature_block * feature_block, axis=1)
    normed = (feature_block * mixer_gain).astype(jnp.bfloat16)
    partial_value = jnp.concatenate(
        [
            jnp.dot(normed, query_weight, preferred_element_type=jnp.float32),
            jnp.dot(normed, key_weight, preferred_element_type=jnp.float32),
            jnp.dot(normed, value_weight, preferred_element_type=jnp.float32),
            jnp.dot(normed, gate_weight, preferred_element_type=jnp.float32),
        ],
        axis=1,
    )
    owned_rows = owned_sums(partial_value, squares)
    local_heads = query_weight.shape[1] // QK
    q_width = query_weight.shape[1]
    v_width = value_weight.shape[1]
    head_width = v_width // local_heads
    seq_rows = owned_rows.shape[0]
    query_rows = rotate_heads(
        owned_rows[:, :q_width].reshape(seq_rows, local_heads, QK), lengths
    ).astype(jnp.bfloat16)
    key_rows = (
        rotate_heads(
            owned_rows[:, q_width : 2 * q_width].reshape(seq_rows, local_heads, QK), lengths
        )
        * QK ** (-0.5)
    ).astype(jnp.bfloat16)
    value_rows = (
        owned_rows[:, 2 * q_width : 2 * q_width + v_width]
        .astype(jnp.bfloat16)
        .reshape(seq_rows, local_heads, head_width)
    )
    gate_rows = owned_rows[:, 2 * q_width + v_width :]
    head_ids = (lax.axis_index("tp") * local_heads + jnp.arange(local_heads)).astype(jnp.float32)
    decay_rate = 1.0 - 2.0 ** (-5.0 - 10.0 * head_ids / (HEADS - 1))
    new_state = (
        decay_rate[None, :, None, None] * retention_state
        + key_rows.astype(jnp.float32)[..., :, None] * value_rows.astype(jnp.float32)[..., None, :]
    )
    retained = jnp.einsum(
        "bhk,bhkv->bhv", query_rows.astype(jnp.float32), new_state, precision=lax.Precision.HIGHEST
    )
    normalized = retained * lax.rsqrt(jnp.mean(retained * retained, axis=-1) + 1e-06)[..., None]
    merged = (normalized.reshape(seq_rows, v_width) * jax.nn.silu(gate_rows)).astype(jnp.bfloat16)
    mixed_part = jnp.dot(
        gather_directly(merged, "kv", 0), output_weight, preferred_element_type=jnp.float32
    )
    mixed_cols = sent_and_summed(mixed_part.astype(jnp.bfloat16), "tp", 1)
    residual = (tokens.astype(jnp.float32) + mixed_cols).astype(jnp.bfloat16)
    block_two = gathered_rows(residual).astype(jnp.float32)
    squares_two = jnp.sum(block_two * block_two, axis=1)
    normed_two = (block_two * channel_gain).astype(jnp.bfloat16)
    partial_two = jnp.concatenate(
        [
            jnp.dot(normed_two, ffn_gate, preferred_element_type=jnp.float32),
            jnp.dot(normed_two, ffn_up, preferred_element_type=jnp.float32),
        ],
        axis=1,
    )
    hidden_units = ffn_gate.shape[1]
    summed = owned_sums(partial_two, squares_two)
    hidden = (jax.nn.silu(summed[:, :hidden_units]) * summed[:, hidden_units:]).astype(jnp.bfloat16)
    down_part = jnp.dot(
        gather_directly(hidden, "kv", 0), ffn_down, preferred_element_type=jnp.float32
    )
    down_sums = sent_and_summed(down_part.astype(jnp.bfloat16), "tp", 1)
    layer_output = (residual.astype(jnp.float32) + down_sums).astype(jnp.bfloat16)
    return (layer_output, new_state)


def solution(mesh):
    in_specs = (
        P(None, ("kv", "tp")),
        P("kv"),
        P("kv", "tp", None, None),
        P("kv"),
        P("kv", "tp"),
        P("kv", "tp"),
        P("kv", "tp"),
        P("kv", "tp"),
        P("tp", "kv"),
        P("kv"),
        P("kv", "tp"),
        P("kv", "tp"),
        P("tp", "kv"),
    )
    out_specs = (P(None, ("kv", "tp")), P("kv", "tp", None, None))
    return jax.shard_map(
        on_device, mesh=mesh, in_specs=in_specs, out_specs=out_specs, check_vma=False
    )
```

profile of v0, /device:TPU:1, one launch (start us, length us, event | category | flops | bytes accessed | tf_op | source)
XLA Modules:
  0.0 126.4 jit_solution(4354620266394448964)
XLA Ops:
  0.6 0.0 copy-start
  0.6 0.0 copy-start.2
  0.7 21.8 %all_gather.6 = bf16[128,256]{0,1:T(8,128)(2,1)S(1)} all-gather(bf16[128,16]{0,1:T(8,128)(2,1)} %param.13), channel_id=1, replica_groups=mesh['kv'=16,'tp'=16] {'tp'}, dimensions={1}, use_global_device_ids=true | all-gather | bytes 69632 | tf_op jit(solution)/shard_map/all_gather | solution.py:67
  22.5 0.1 fusion.12
  22.6 0.2 convert_element_type.141
  22.8 1.8 %fusion.5 = bf16[16,8,769]{2,1,0:T(8,128)(2,1)} fusion(bf16[256,128]{1,0:T(8,128)(2,1)} %param.17, bf16[128,256]{0,1:T(8,128)(2,1)S(1)} %all_gather.6, f32[256]{0:T(256)} %param.16), kind=kOutput, calls=%fused_computation.13 | convolution fusion | flops 8503295 | bytes 164864 | tf_op jit(solution)/shard_map/dot_general | solution.py:98
  24.6 1.8 %fusion.7 = bf16[16,8,769]{2,1,0:T(8,128)(2,1)} fusion(bf16[16,8,769]{2,1,0:T(8,128)(2,1)} %fusion.5, bf16[256,128]{1,0:T(8,128)(2,1)} %param.18, bf16[128,256]{0,1:T(8,128)(2,1)S(1)} %all_gather.6, f32[256]{0:T(256)} %param.16), kind=kOutput, calls=%fused_computation.15 | convolution fusion | flops 8503296 | bytes 164864 | tf_op jit(solution)/shard_map/dot_general | solution.py:99
  26.3 1.8 %fusion.1 = bf16[16,8,769]{2,1,0:T(8,128)(2,1)} fusion(bf16[16,8,769]{2,1,0:T(8,128)(2,1)} %fusion.7, bf16[256,256]{1,0:T(8,128)(2,1)} %param.19, bf16[128,256]{0,1:T(8,128)(2,1)S(1)} %all_gather.6, f32[256]{0:T(256)} %param.16), kind=kOutput, calls=%fused_computation.7 | convolution fusion | flops 16908288 | bytes 263168 | tf_op jit(solution)/shard_map/dot_general | solution.py:100
  28.1 1.8 %fusion.3 = bf16[16,8,769]{2,1,0:T(8,128)(2,1)} fusion(bf16[16,8,769]{2,1,0:T(8,128)(2,1)} %fusion.1, bf16[256,256]{1,0:T(8,128)(2,1)} %param.20, bf16[128,256]{0,1:T(8,128)(2,1)S(1)} %all_gather.6, f32[256]{0:T(256)} %param.16), kind=kOutput, calls=%fused_computation.9 | convolution fusion | flops 16908288 | bytes 263168 | tf_op jit(solution)/shard_map/dot_general | solution.py:101
  30.0 0.6 constant_dynamic-update-slice_fusion
  30.6 6.8 %all-to-all-start = ((bf16[16,8,769]{2,1,0:T(8,128)(2,1)}), bf16[16,8,769]{2,1,0:T(8,128)(2,1)S(1)}, u32[]{:S(2)}, u32[]{:S(2)}) async-start(bf16[16,8,769]{2,1,0:T(8,128)(2,1)} %constant_dynamic-update-slice_fusion), calls=%async_computation | async-start | bytes 458752 | tf_op jit(solution)/shard_map/all_to_all | solution.py:19
  37.4 0.0 copy-start.8
  37.4 0.6 copy-done.8
  38.1 7.3 %all-to-all-done = bf16[16,8,769]{2,1,0:T(8,128)(2,1)S(1)} async-done(((bf16[16,8,769]{2,1,0:T(8,128)(2,1)}), bf16[16,8,769]{2,1,0:T(8,128)(2,1)S(1)}, u32[]{:S(2)}, u32[]{:S(2)}) %all-to-all-start) | async-done | bytes 196896 | tf_op jit(solution)/shard_map/all_to_all | solution.py:19
  45.4 0.1 fusion.44
  45.5 0.1 slice_multiply_fusion.2
  45.6 0.1 fusion.49
  45.7 0.1 maximum_bitcast_fusion
  45.8 0.1 fusion.47
  45.9 0.0 copy-done.2
  45.9 0.2 multiply_add_fusion
  46.1 0.0 copy-start.1
  46.1 0.5 fusion.8
  46.6 0.0 copy-start.5
  46.6 0.1 fusion.19
  46.7 0.1 fusion.21
  46.8 9.2 %all_to_all.30 = bf16[16,8,256]{2,1,0:T(8,128)(2,1)S(1)} all-to-all(bf16[16,8,256]{2,1,0:T(8,128)(2,1)S(1)} %broadcast_in_dim.4), channel_id=1, replica_groups=mesh['kv'=16,'tp'=16] {'kv'}, dimensions={0} | all-to-all | bytes 131072 | tf_op jit(solution)/shard_map/all_to_all | solution.py:36
  55.9 0.0 copy-done.5
  56.0 0.2 convolution_convert_fusion.3
  56.1 0.1 copy.37
  56.2 13.9 %all_to_all.31 = bf16[16,128,16]{1,2,0:T(8,128)(2,1)S(1)} all-to-all(bf16[16,128,16]{1,2,0:T(8,128)(2,1)S(1)} %bitcast.66), channel_id=1, replica_groups=mesh['kv'=16,'tp'=16] {'tp'}, dimensions={0} | all-to-all | bytes 131072 | tf_op jit(solution)/shard_map/all_to_all | solution.py:19
  70.2 0.0 copy-start.6
  70.2 0.7 copy-done.6
  70.9 14.9 %all_gather.7 = bf16[128,256]{0,1:T(8,128)(2,1)S(1)} all-gather(bf16[128,16]{0,1:T(8,128)(2,1)S(1)} %add_convert_fusion.1), channel_id=1, replica_groups=mesh['kv'=16,'tp'=16] {'tp'}, dimensions={1}, use_global_device_ids=true | all-gather | bytes 69632 | tf_op jit(solution)/shard_map/all_gather | solution.py:67
  85.7 0.1 fusion.14
  85.8 0.0 copy-start.7
  85.8 0.2 convert_element_type.142
  86.0 0.0 copy-done
  86.0 0.4 copy-done.7
  86.5 0.0 copy-start.3
  86.5 0.3 convolution_convert_fusion.1
  86.8 0.0 copy-done.1
  86.8 0.1 copy.38
  86.9 0.5 copy-done.3
  87.4 0.3 convolution_convert_fusion
  87.8 0.1 copy.39
  87.9 0.2 concatenate.65
  88.1 12.3 %all_to_all.32 = bf16[16,8,1409]{2,1,0:T(8,128)(2,1)S(1)} all-to-all(bf16[16,8,1409]{2,1,0:T(8,128)(2,1)S(1)} %concatenate.65), channel_id=1, replica_groups=mesh['kv'=16,'tp'=16] {'kv'}, dimensions={0} | all-to-all | bytes 721408 | tf_op jit(solution)/shard_map/all_to_all | solution.py:19
  100.4 0.1 convert_reduce_fusion
  100.5 0.1 fusion.41
  100.6 0.0 copy-start.4
  100.6 0.1 slice_multiply_fusion
  100.7 0.1 fusion.18
  100.8 10.4 %all_to_all.33 = bf16[16,8,704]{2,1,0:T(8,128)(2,1)S(1)} all-to-all(bf16[16,8,704]{2,1,0:T(8,128)(2,1)S(1)} %broadcast_in_dim.5), channel_id=1, replica_groups=mesh['kv'=16,'tp'=16] {'kv'}, dimensions={0} | all-to-all | bytes 360448 | tf_op jit(solution)/shard_map/all_to_all | solution.py:36
  111.1 0.0 copy-done.4
  111.1 0.2 convolution_convert_fusion.2
  111.4 0.1 copy.41
  111.5 14.3 %all_to_all.34 = bf16[16,128,16]{1,2,0:T(8,128)(2,1)S(1)} all-to-all(bf16[16,128,16]{1,2,0:T(8,128)(2,1)S(1)} %bitcast.67), channel_id=1, replica_groups=mesh['kv'=16,'tp'=16] {'tp'}, dimensions={0} | all-to-all | bytes 131072 | tf_op jit(solution)/shard_map/all_to_all | solution.py:19
  125.8 0.6 add_convert_fusion
  (11 shorter events, 0.1 us)
Async XLA Ops:
  0.6 85.4 %copy-start = (bf16[256,704]{0,1:T(8,128)(2,1)S(1)}, bf16[256,704]{0,1:T(8,128)(2,1)}, u32[]{:S(2)}) copy-start(bf16[256,704]{0,1:T(8,128)(2,1)} %param.23) | copy-start | bytes 1081348
  0.6 45.2 %copy-start.2 = (f32[8,1,128,256]{3,2,1,0:T(8,128)S(1)}, f32[8,1,128,256]{3,2,1,0:T(8,128)}, u32[]{:S(2)}) copy-start(f32[8,1,128,256]{3,2,1,0:T(8,128)} %param.15) | copy-start | bytes 3145732
  30.6 14.7 %all-to-all-start = ((bf16[16,8,769]{2,1,0:T(8,128)(2,1)}), bf16[16,8,769]{2,1,0:T(8,128)(2,1)S(1)}, u32[]{:S(2)}, u32[]{:S(2)}) async-start(bf16[16,8,769]{2,1,0:T(8,128)(2,1)} %constant_dynamic-update-slice_fusion), calls=%async_computation | async-start | bytes 458752 | tf_op jit(solution)/shard_map/all_to_all | solution.py:19
  37.4 0.7 copy-start.8
  46.1 40.7 %copy-start.1 = (f32[8,1,128,256]{3,2,1,0:T(8,128)}, f32[8,1,128,256]{3,2,1,0:T(8,128)S(1)}, u32[]{:S(2)}) copy-start(f32[8,1,128,256]{3,2,1,0:T(8,128)S(1)} %multiply_add_fusion) | copy-start | bytes 3145732
  46.6 9.4 %copy-start.5 = (bf16[256,256]{1,0:T(8,128)(2,1)S(1)}, bf16[256,256]{1,0:T(8,128)(2,1)}, u32[]{:S(2)}) copy-start(bf16[256,256]{1,0:T(8,128)(2,1)} %param.21) | copy-start | bytes 393220
  70.2 0.7 copy-start.6
  85.8 0.7 copy-start.7
  86.5 1.0 copy-start.3
  100.6 10.6 %copy-start.4 = (bf16[704,256]{1,0:T(8,128)(2,1)S(1)}, bf16[704,256]{1,0:T(8,128)(2,1)}, u32[]{:S(2)}) copy-start(bf16[704,256]{1,0:T(8,128)(2,1)} %param.25) | copy-start | bytes 1081348
where the time goes:
time: 127 us; the launch traced here: 126 us
  blocking collectives  96.8 us (76%)
  matrix products  8.66 us (7%)
  waiting for transfers between devices  7.25 us (6%)
  starting transfers between devices  6.75 us (5%)
  local copies, waits for them, and re-layouts  4.08 us (3%)
  other arithmetic  1.99 us (2%)
    all_to_all x3, blocking collectives, sent_and_summed(): lax.all_to_all(blocks, axis, split_axis=0, concat_axis=0, tiled=True)  40.5 us
    all_gather x2, blocking collectives, gathered_rows(): return lax.all_gather(columns, 'tp', axis=1, tiled=True)  36.7 us
    all_to_all x2, blocking collectives, copy_for_each(): lax.all_to_all(jnp.broadcast_to(value[None], (devices, *value.shape)), ax...  19.6 us
    all_to_all x1, waiting for transfers between devices, sent_and_summed(): lax.all_to_all(blocks, axis, split_axis=0, concat_axis=0, tiled=True)  7.25 us
    all_to_all x1, starting transfers between devices, sent_and_summed(): lax.all_to_all(blocks, axis, split_axis=0, concat_axis=0, tiled=True)  6.75 us
  transfers between devices with their start and end apart: 1, of which 1 were waited for; matrix products, arithmetic and copies ran while one was open for 0% of the time, Pallas kernels for 0%

commit v1 on v0

v1 whole, which is shorter than its diff:
```python
import math

import jax
import jax.numpy as jnp
from jax import lax
from jax.experimental import pallas as pl
from jax.experimental.pallas import tpu as pltpu
from jax.sharding import PartitionSpec as P

D = 4096
HEADS = 16
QK = 128
VD = 256
LANES = 128
F32 = jnp.float32
BF16 = jnp.bfloat16
VMEM_BYTES = 8 << 20
FULL_VMEM_BYTES = 67_043_328 - 1_000_000


def local_call(kernel, outs, *operands, scratch=(), space=pltpu.VMEM, limit=VMEM_BYTES):
    spaces = [space] * len(operands)
    several = isinstance(outs, tuple)
    vmem = pl.BlockSpec(memory_space=pltpu.VMEM)
    return pl.pallas_call(
        kernel,
        out_shape=outs,
        in_specs=[pl.BlockSpec(memory_space=s) for s in spaces],
        out_specs=tuple(vmem for _ in outs) if several else vmem,
        scratch_shapes=scratch,
        compiler_params=pltpu.CompilerParams(vmem_limit_bytes=limit),
    )(*operands)


def shaped(shape, dtype):
    return pltpu.VMEM(shape, dtype)


def store_rows(out_ref, value, start):
    each = out_ref.shape[1]
    for owner in range(out_ref.shape[0]):
        out_ref[owner, :, start : start + value.shape[1]] = value[
            owner * each : (owner + 1) * each
        ].astype(out_ref.dtype)


def all_rows(ref):
    return jnp.concatenate([ref[i].astype(F32) for i in range(ref.shape[0])], axis=0)


def summed(ref):
    total = ref[0].astype(F32)
    for i in range(1, ref.shape[0]):
        total = total + ref[i].astype(F32)
    return total


def prepare(token_ref, length_ref, *refs):
    count = (len(refs) - 6) // 2
    sources, (copies_ref, sine_ref, cosine_ref), fetched = (
        refs[:count],
        refs[count : count + 3],
        refs[count + 3 : 2 * count + 3],
    )
    tokens_vmem, lengths_smem, sems = refs[2 * count + 3 :]
    copies = [
        pltpu.make_async_copy(source, target, sems.at[i])
        for i, (source, target) in enumerate(
            zip((token_ref, length_ref, *sources), (tokens_vmem, lengths_smem, *fetched))
        )
    ]
    for copy in copies:
        copy.start()
    copies[1].wait()
    shape = sine_ref.shape
    row = lax.broadcasted_iota(jnp.int32, shape, 0)
    position = jnp.zeros(shape, F32)
    for i in range(shape[0]):
        position = jnp.where(row == i, lengths_smem[i].astype(F32), position)
    sine, cosine = sine_cosine(position * frequencies(shape))
    first = lax.broadcasted_iota(jnp.int32, shape, 1) < QK // 2
    sine_ref[...] = jnp.where(first, -sine, sine)
    cosine_ref[...] = cosine
    copies[0].wait()
    tokens = tokens_vmem[...]
    for i in range(copies_ref.shape[0]):
        copies_ref[i] = tokens
    for copy in copies[2:]:
        copy.wait()


def project(x_ref, gain_ref, q_ref, k_ref, v_ref, g_ref, out_ref, half_ref):
    x = x_ref[...].astype(F32).reshape(-1, x_ref.shape[2]).T
    normed = (x * gain_ref[...].reshape(1, -1)).astype(BF16)
    at = 0
    for w_ref in (q_ref, k_ref, v_ref, g_ref):
        store_rows(out_ref, jnp.dot(normed, w_ref[...], preferred_element_type=F32), at)
        at += w_ref.shape[1]
    squares = jnp.sum(x * x, axis=1, keepdims=True)
    store_rows(out_ref, jnp.broadcast_to(squares, (x.shape[0], LANES)), at)
    core = lax.rem(lax.axis_index("tp"), 2)
    width = half_ref.shape[1]
    half_ref[...] = jnp.where(core == 0, x[:, :width], x[:, width:]).astype(BF16)


def frequencies(shape):
    lane = lax.broadcasted_iota(jnp.int32, shape, 1)
    result = jnp.ones(shape, F32)
    for bit in range(6):
        factor = 10000.0 ** (-(2.0**bit) / (QK // 2))
        result = jnp.where((lane >> bit) & 1 == 1, result * F32(factor), result)
    return result


def sine_cosine(angle):
    turns = jnp.floor(angle * F32(2.0 / math.pi) + 0.5)
    rest = angle - turns * F32(1.5703125)
    rest = rest - turns * F32(4.837512969970703125e-4)
    rest = rest - turns * F32(7.54978995489188216e-8)
    square = rest * rest
    sine = rest + rest * square * (
        F32(-1.6666654611e-1) + square * (F32(8.3321608736e-3) + square * F32(-1.9515295891e-4))
    )
    cosine = (
        1.0
        - 0.5 * square
        + square
        * square
        * (
            F32(4.166664568298827e-2)
            + square * (F32(-1.388731625493765e-3) + square * F32(2.443315711809948e-5))
        )
    )
    quarter = turns.astype(jnp.int32) & 3
    odd = (quarter & 1) == 1
    first, second = jnp.where(odd, cosine, sine), jnp.where(odd, sine, cosine)
    return (
        jnp.where(quarter >= 2, -first, first),
        jnp.where((quarter == 1) | (quarter == 2), -second, second),
    )


def retain(parts_ref, sine_ref, cosine_ref, state_ref, out_ref, new_ref):
    sums = summed(parts_ref)
    rows = sums.shape[0]
    scale = lax.rsqrt(sums[:, 2 * QK + 2 * VD :] / D + 1e-06)
    wide_scale = jnp.concatenate([scale, scale], axis=1)
    signed, cosine = sine_ref[...], cosine_ref[...]

    def rotated(vectors):
        return vectors * cosine + pltpu.roll(vectors, QK // 2, 1) * signed

    query = rotated(sums[:, :QK] * scale).astype(BF16).astype(F32)
    key = (rotated(sums[:, QK : 2 * QK] * scale) * QK ** (-0.5)).astype(BF16).astype(F32)
    value = (sums[:, 2 * QK : 2 * QK + VD] * wide_scale).astype(BF16).astype(F32)
    gate = sums[:, 2 * QK + VD : 2 * QK + 2 * VD] * wide_scale
    columns = jnp.concatenate([query, key] * (QK // (2 * rows)), axis=0).T
    head = jnp.full((1, VD), lax.axis_index("tp"), jnp.int32).astype(F32)
    decay = 1.0 - jnp.exp2(-5.0 - 10.0 * head / (HEADS - 1))
    retained = []
    for i in range(rows):
        state = (
            decay * state_ref[i, 0]
            + columns[:, rows + i : rows + i + 1] * value[i : i + 1]
        )
        new_ref[i, 0] = state
        retained.append(jnp.sum(state * columns[:, i : i + 1], axis=0, keepdims=True))
    retained = jnp.concatenate(retained, axis=0)
    inverse = lax.rsqrt(jnp.mean(retained * retained, axis=1, keepdims=True) + 1e-06)
    merged = (retained * inverse * (gate / (1.0 + jnp.exp(-gate)))).astype(BF16)
    for i in range(out_ref.shape[0]):
        out_ref[i] = merged


def mix(merged_ref, w_ref, kept_ref, given_ref):
    mixed = jnp.dot(
        all_rows(merged_ref).astype(BF16), w_ref[...], preferred_element_type=F32
    )
    width = kept_ref.shape[1]
    low, high = mixed[:, :width], mixed[:, width:]
    first = lax.rem(lax.axis_index("tp"), 2) == 0
    kept_ref[...] = jnp.where(first, low, high)
    given_ref[...] = jnp.where(first, high, low).astype(BF16)


def add_given(kept_ref, given_ref, out_ref):
    total = (kept_ref[...] + given_ref[...].astype(F32)).astype(BF16)
    for i in range(out_ref.shape[0]):
        out_ref[i] = total


def add_chips(parts_ref, token_ref, out_ref):
    out_ref[...] = (token_ref[...].astype(F32) + summed(parts_ref)).astype(BF16)


def expand(half_ref, other_ref, gain_ref, gate_ref, up_ref, out_ref, mine_ref, flipped_ref):
    me = lax.axis_index("tp")
    first = lax.rem(me, 2) == 0
    half, other = half_ref[...].astype(F32), other_ref[...].astype(F32)
    x = jnp.concatenate(
        [jnp.where(first, half, other), jnp.where(first, other, half)], axis=1
    )
    normed = (x * gain_ref[...].reshape(1, -1)).astype(BF16)
    contract = (((1,), (1,)), ((), ()))
    units = gate_ref.shape[0]
    gate = lax.dot_general(normed, gate_ref[...], contract, preferred_element_type=F32)
    up = lax.dot_general(normed, up_ref[...], contract, preferred_element_type=F32)
    spare = out_ref.shape[2] // 2 - units
    squares = jnp.broadcast_to(jnp.sum(x * x, axis=1, keepdims=True), (x.shape[0], spare))
    store_rows(out_ref, jnp.concatenate([gate, squares, up, squares], axis=1), 0)
    flipped_ref[...] = x.T
    width = mine_ref.shape[0]
    mine_ref[...] = flipped_ref[pl.ds(pl.multiple_of(me * width, width), width), :]


def activate(parts_ref, out_ref):
    sums = summed(parts_ref)
    units, middle = out_ref.shape[2], sums.shape[1] // 2
    scale = lax.rsqrt(sums[:, units : units + 1] / D + 1e-06)
    gate = sums[:, :units] * scale
    up = sums[:, middle : middle + units] * scale
    hidden = (gate / (1.0 + jnp.exp(-gate)) * up).astype(BF16)
    for i in range(out_ref.shape[0]):
        out_ref[i] = hidden


def contract_units(hidden_ref, w_ref, out_ref):
    down = jnp.dot(all_rows(hidden_ref).astype(BF16), w_ref[...], preferred_element_type=F32)
    out_ref[...] = down.T.astype(BF16).reshape(out_ref.shape)


def finish(parts_ref, mine_ref, out_ref):
    out_ref[...] = (mine_ref[...] + summed(parts_ref)).astype(BF16)


def exchanged(blocks, axis, groups=None):
    return lax.all_to_all(blocks, axis, 0, 0, tiled=True, axis_index_groups=groups)


def on_device(
    tokens,
    lengths,
    retention_state,
    mixer_gain,
    query_weight,
    key_weight,
    value_weight,
    gate_weight,
    output_weight,
    channel_gain,
    ffn_gate,
    ffn_up,
    ffn_down,
):
    owners, members = lax.axis_size("kv"), lax.axis_size("tp")
    batch, own_width = tokens.shape
    rows = batch // owners
    block = own_width * members
    half = block // 2
    units = ffn_gate.shape[1]
    middle = -(-(units + 1) // LANES) * LANES
    swap = [(i, i ^ 1) for i in range(members)]
    along_z = [[i + c for i in range(0, members, 2)] for c in range(2)]

    weights = (query_weight, key_weight, value_weight, gate_weight)
    fetch = (mixer_gain, channel_gain, *weights)
    copies, sine, cosine, mixer_gain, channel_gain, *weights = local_call(
        prepare,
        (
            shaped((members, own_width, batch), BF16),
            shaped((rows, QK), F32),
            shaped((rows, QK), F32),
            *(shaped(a.shape, a.dtype) for a in fetch),
        ),
        tokens.T,
        lengths,
        *fetch,
        scratch=(
            pltpu.VMEM((own_width, batch), BF16),
            pltpu.SMEM((rows,), jnp.int32),
            pltpu.SemaphoreType.DMA((len(fetch) + 2,)),
        ),
        space=pltpu.HBM,
        limit=FULL_VMEM_BYTES,
    )
    features = exchanged(copies, "tp")
    width = 2 * QK + 2 * VD + LANES
    parts, token_half = local_call(
        project,
        (shaped((owners, rows, width), BF16), shaped((batch, half), BF16)),
        features,
        mixer_gain,
        *weights,
    )
    merged, new_state = local_call(
        retain,
        (shaped((owners, rows, VD), BF16), shaped(retention_state.shape, F32)),
        exchanged(parts, "kv"),
        sine,
        cosine,
        retention_state,
    )
    kept, given = local_call(
        mix,
        (shaped((batch, half), F32), shaped((batch, half), BF16)),
        exchanged(merged, "kv"),
        output_weight,
    )
    chip_sum = local_call(
        add_given,
        shaped((members // 2, batch, half), BF16),
        kept,
        lax.ppermute(given, "tp", swap),
    )
    residual_half = local_call(
        add_chips,
        shaped((batch, half), BF16),
        exchanged(chip_sum, "tp", along_z),
        token_half,
    )
    parts, mine = local_call(
        expand,
        (shaped((owners, rows, 2 * middle), BF16), shaped((own_width, batch), F32)),
        residual_half,
        lax.ppermute(residual_half, "tp", swap),
        channel_gain,
        ffn_gate.T,
        ffn_up.T,
        scratch=(pltpu.VMEM((block, batch), F32),),
    )
    hidden = local_call(
        activate, shaped((owners, rows, units), BF16), exchanged(parts, "kv")
    )
    down = local_call(
        contract_units,
        shaped((members, own_width, batch), BF16),
        exchanged(hidden, "kv"),
        ffn_down,
    )
    layer_output = local_call(
        finish, jax.ShapeDtypeStruct((own_width, batch), BF16), exchanged(down, "tp"), mine
    )
    return (layer_output.T, new_state)


def solution(mesh):
    in_specs = (
        P(None, ("kv", "tp")),
        P("kv"),
        P("kv", "tp", None, None),
        P("kv"),
        P("kv", "tp"),
        P("kv", "tp"),
        P("kv", "tp"),
        P("kv", "tp"),
        P("tp", "kv"),
        P("kv"),
        P("kv", "tp"),
        P("kv", "tp"),
        P("tp", "kv"),
    )
    out_specs = (P(None, ("kv", "tp")), P("kv", "tp", None, None))
    return jax.shard_map(
        on_device, mesh=mesh, in_specs=in_specs, out_specs=out_specs, check_vma=False
    )
```

time: 127 us -> 103 us (0.81)
  blocking collectives: 96.8 us -> 79 us
  matrix products: 8.66 us -> 0 us
  Pallas kernels: 0 us -> 4.22 us
  local copies, waits for them, and re-layouts: 4.08 us -> 1 us
  starting transfers between devices: 6.75 us -> 9.2 us
  other arithmetic: 1.99 us -> 0 us
  waiting for transfers between devices: 7.25 us -> 8.57 us
    all_gather x2 -> x0, blocking collectives: 36.7 us -> none  [gathered_rows(): return lax.all_gather(columns, 'tp', axis=1, tiled=True)]
    all_to_all x5 -> x6, blocking collectives: 60.1 us -> 79 us  [exchanged(): lax.all_to_all(blocks, axis, 0, 0, tiled=True, axis_index_groups=groups)]
    dot_general x9 -> x0, matrix products: 8.66 us -> none  [the longest x1 1.83 us: on_device(): jnp.dot(normed, value_weight, preferred_element_type=jnp.float32)]
    pallas_call x0 -> x10, Pallas kernels: none -> 4.22 us  [local_call(): pl.pallas_call(kernel, out_shape=outs, in_specs=[pl.BlockSpec(memory_spac...]
    ppermute x0 -> x2, starting transfers between devices: none -> 3.33 us  [the longest x1 2.76 us: on_device(): lax.ppermute(given, 'tp', swap)]
    ppermute x0 -> x2, waiting for transfers between devices: none -> 1.72 us  [the longest x1 0.86 us: on_device(): lax.ppermute(given, 'tp', swap)]
    unnamed x18 -> x11, local copies, waits for them, and re-layouts: 2.27 us -> 1 us
  transfers between devices with their start and end apart: 1 -> 3, of which waited for: 1 -> 3; matrix products, arithmetic and copies ran while one was open for 0% -> 1% of each run, Pallas kernels for 0% -> 0%
where the time goes in v1:
time: 103 us
  blocking collectives  79 us (77%)
  starting transfers between devices  9.2 us (9%)
  waiting for transfers between devices  8.57 us (8%)
  Pallas kernels  4.22 us (4%)
    all_to_all x6, blocking collectives, exchanged(): lax.all_to_all(blocks, axis, 0, 0, tiled=True, axis_index_groups=groups)  79 us
    all_to_all x1, waiting for transfers between devices, exchanged(): lax.all_to_all(blocks, axis, 0, 0, tiled=True, axis_index_groups=groups)  6.85 us
    all_to_all x1, starting transfers between devices, exchanged(): lax.all_to_all(blocks, axis, 0, 0, tiled=True, axis_index_groups=groups)  5.87 us
    pallas_call x10, Pallas kernels, local_call(): pl.pallas_call(kernel, out_shape=outs, in_specs=[pl.BlockSpec(memory_spac...  4.22 us
    ppermute x1, starting transfers between devices, on_device(): lax.ppermute(given, 'tp', swap)  2.76 us
  transfers between devices with their start and end apart: 3, of which 3 were waited for; matrix products, arithmetic and copies ran while one was open for 1% of the time, Pallas kernels for 0%

profile of v1, /device:TPU:1, one launch (start us, length us, event | category | flops | bytes accessed | tf_op | source)
XLA Modules:
  0.0 102.7 jit_solution(211631702590564054)
XLA Ops:
  0.6 1.2 %shard_map.140 = (bf16[16,16,128]{2,1,0:T(8,128)(2,1)S(1)}, f32[8,128]{1,0:T(8,128)S(1)}, f32[8,128]{1,0:T(8,128)S(1)}, f32[256]{0:T(256)S(1)}, f32[256]{0:T(256...) custom-call(bf16[16,128]{1,0:T(8,128)(2,1)} %bitcast.6, ...), custom_call_target="tpu_custom_call" | custom-call | tf_op jit(solution)/shard_map/pallas_call | solution.py:25
  1.8 0.0 copy-start
  1.8 17.7 %all_to_all.35.x_ref = bf16[16,16,128]{2,1,0:T(8,128)(2,1)S(1)} all-to-all(bf16[16,16,128]{2,1,0:T(8,128)(2,1)S(1)} %get-tuple-element.19), channel_id=1, replica_groups=mesh['kv'=16,'tp'=16] {'tp'}, dimensions={0} | all-to-all | bytes 131072 | tf_op jit(solution)/shard_map/all_to_all | solution.py:237
  19.5 0.3 shard_map.141
  19.8 14.6 %all_to_all.36.parts_ref = bf16[16,8,896]{2,1,0:T(8,128)(2,1)S(1)} all-to-all(bf16[16,8,896]{2,1,0:T(8,128)(2,1)S(1)} %get-tuple-element.25), channel_id=1, replica_groups=mesh['kv'=16,'tp'=16] {'kv'}, dimensions={0} | all-to-all | bytes 458752 | tf_op jit(solution)/shard_map/all_to_all | solution.py:237
  34.3 0.0 copy-done
  34.4 0.5 shard_map.142
  34.9 0.0 copy-start.4
  34.9 9.3 %all_to_all.37.merged_ref = bf16[16,8,256]{2,1,0:T(8,128)(2,1)S(1)} all-to-all(bf16[16,8,256]{2,1,0:T(8,128)(2,1)S(1)} %get-tuple-element.28), channel_id=1, replica_groups=mesh['kv'=16,'tp'=16] {'kv'}, dimensions={0} | all-to-all | bytes 131072 | tf_op jit(solution)/shard_map/all_to_all | solution.py:237
  44.2 0.0 copy-done.4
  44.2 0.2 shard_map.143
  44.4 2.8 %collective-permute-start = (bf16[128,128]{1,0:T(8,128)(2,1)S(1)}, bf16[128,128]{1,0:T(8,128)(2,1)S(1)}, u32[]{:S(2)}, u32[]{:S(2)}) collective-permute-start(bf16[128,128]{1,0:T(8,128)(2,1)S(1)} %get-tuple-element.30), channel_id=1, source_target_pairs={{0,1},{1,0},{2,3},{3,2},{4,5},{5,4},{6,7},{7,6},{8,9},{9,8},{10,11... | collective-permute-start | bytes 98312 | tf_op jit(solution)/shard_map/ppermute | solution.py:313
  47.2 0.9 collective-permute-done.given_ref
  48.0 0.0 copy-start.1
  48.1 0.0 copy-start.2
  48.1 14.9 %all_to_all.38.parts_ref = bf16[8,128,128]{2,1,0:T(8,128)(2,1)S(1)} all-to-all(bf16[8,128,128]{2,1,0:T(8,128)(2,1)S(1)} %shard_map.144), channel_id=1, replica_groups={{0,2,4,6,8,10,12,14},{1,3,5,7,9,11,13,15},{16,18,20,22,24,26,28,30},{17..., dimensions={0} | all-to-all | bytes 524288 | tf_op jit(solution)/shard_map/all_to_all | solution.py:237
  63.0 0.6 collective-permute-start.1
  63.6 0.9 collective-permute-done.1.other_ref
  64.4 0.0 copy-done.1
  64.4 0.0 copy-done.2
  64.4 0.4 shard_map.146
  64.8 12.4 %all_to_all.39.parts_ref = bf16[16,8,1536]{2,1,0:T(8,128)(2,1)S(1)} all-to-all(bf16[16,8,1536]{2,1,0:T(8,128)(2,1)S(1)} %get-tuple-element.33), channel_id=1, replica_groups=mesh['kv'=16,'tp'=16] {'kv'}, dimensions={0} | all-to-all | bytes 786432 | tf_op jit(solution)/shard_map/all_to_all | solution.py:237
  77.2 0.0 copy-start.3
  77.2 0.1 shard_map.147
  77.3 10.1 %all_to_all.40.hidden_ref = bf16[16,8,704]{2,1,0:T(8,128)(2,1)S(1)} all-to-all(bf16[16,8,704]{2,1,0:T(8,128)(2,1)S(1)} %shard_map.147), channel_id=1, replica_groups=mesh['kv'=16,'tp'=16] {'kv'}, dimensions={0} | all-to-all | bytes 360448 | tf_op jit(solution)/shard_map/all_to_all | solution.py:237
  87.5 0.0 copy-done.3
  87.5 0.9 shard_map.148
  88.4 5.9 %all-to-all-start.6 = ((bf16[16,16,128]{2,1,0:T(8,128)(2,1)}), bf16[16,16,128]{2,1,0:T(8,128)(2,1)S(1)}, u32[]{:S(2)}, u32[]{:S(2)}) async-start(bf16[16,16,128]{2,1,0:T(8,128)(2,1)} %shard_map.148), calls=%async_computation.6 | async-start | bytes 131072 | tf_op jit(solution)/shard_map/all_to_all | solution.py:237
  94.3 1.0 copy.15
  95.3 6.9 %all-to-all-done.6.parts_ref = bf16[16,16,128]{2,1,0:T(8,128)(2,1)S(1)} async-done(((bf16[16,16,128]{2,1,0:T(8,128)(2,1)}), bf16[16,16,128]{2,1,0:T(8,128)(2,1)S(1)}, u32[]{:S(2)}, u32[]{:S(2)}) %all-to-all-start.6) | async-done | bytes 65568 | tf_op jit(solution)/shard_map/all_to_all | solution.py:237
  102.1 0.6 shard_map.149
  (2 shorter events, 0.1 us)
Async XLA Ops:
  1.8 32.6 %copy-start = (f32[8,1,128,256]{3,2,1,0:T(8,128)S(1)}, f32[8,1,128,256]{3,2,1,0:T(8,128)}, u32[]{:S(2)}) copy-start(f32[8,1,128,256]{3,2,1,0:T(8,128)} %state_ref.1) | copy-start | bytes 3145732
  34.9 9.3 %copy-start.4 = (bf16[256,256]{1,0:T(8,128)(2,1)S(1)}, bf16[256,256]{1,0:T(8,128)(2,1)}, u32[]{:S(2)}) copy-start(bf16[256,256]{1,0:T(8,128)(2,1)} %w_ref.2) | copy-start | bytes 393220
  44.4 3.6 %collective-permute-start = (bf16[128,128]{1,0:T(8,128)(2,1)S(1)}, bf16[128,128]{1,0:T(8,128)(2,1)S(1)}, u32[]{:S(2)}, u32[]{:S(2)}) collective-permute-start(bf16[128,128]{1,0:T(8,128)(2,1)S(1)} %get-tuple-element.30), channel_id=1, source_target_pairs={{0,1},{1,0},{2,3},{3,2},{4,5},{5,4},{6,7},{7,6},{8,9},{9,8},{10,11... | collective-permute-start | bytes 98312 | tf_op jit(solution)/shard_map/ppermute | solution.py:313
  48.0 16.4 %copy-start.1 = (bf16[256,704]{0,1:T(8,128)(2,1)S(1)}, bf16[256,704]{0,1:T(8,128)(2,1)}, u32[]{:S(2)}) copy-start(bf16[256,704]{0,1:T(8,128)(2,1)} %param.23) | copy-start | bytes 1081348
  48.1 16.4 %copy-start.2 = (bf16[256,704]{0,1:T(8,128)(2,1)S(1)}, bf16[256,704]{0,1:T(8,128)(2,1)}, u32[]{:S(2)}) copy-start(bf16[256,704]{0,1:T(8,128)(2,1)} %param.24) | copy-start | bytes 1081348
  63.0 1.4 %collective-permute-start.1 = (bf16[128,128]{1,0:T(8,128)(2,1)S(1)}, bf16[128,128]{1,0:T(8,128)(2,1)S(1)}, u32[]{:S(2)}, u32[]{:S(2)}) collective-permute-start(bf16[128,128]{1,0:T(8,128)(2,1)S(1)} %shard_map.145.half_ref), channel_id=1, source_target_pairs={{0,1},{1,0},{2,3},{3,2},{4,5},{5,4},{6,7},{7,6},{8,9},{9,8},{10,11... | collective-permute-start | bytes 98312 | tf_op jit(solution)/shard_map/ppermute | solution.py:325
  77.2 10.3 %copy-start.3 = (bf16[704,256]{1,0:T(8,128)(2,1)S(1)}, bf16[704,256]{1,0:T(8,128)(2,1)}, u32[]{:S(2)}) copy-start(bf16[704,256]{1,0:T(8,128)(2,1)} %w_ref.3) | copy-start | bytes 1081348
  88.4 13.7 %all-to-all-start.6 = ((bf16[16,16,128]{2,1,0:T(8,128)(2,1)}), bf16[16,16,128]{2,1,0:T(8,128)(2,1)S(1)}, u32[]{:S(2)}, u32[]{:S(2)}) async-start(bf16[16,16,128]{2,1,0:T(8,128)(2,1)} %shard_map.148), calls=%async_computation.6 | async-start | bytes 131072 | tf_op jit(solution)/shard_map/all_to_all | solution.py:237

commit v2 on v1

--- a/solution.py
+++ b/solution.py
@@ -18,10 +18,10 @@
 FULL_VMEM_BYTES = 67_043_328 - 1_000_000
 
 
-def local_call(kernel, outs, *operands, scratch=(), space=pltpu.VMEM, limit=VMEM_BYTES):
+def local_call(kernel, outs, *operands, scratch=(), space=pltpu.VMEM, out_space=pltpu.VMEM, limit=VMEM_BYTES):
     spaces = [space] * len(operands)
     several = isinstance(outs, tuple)
-    vmem = pl.BlockSpec(memory_space=pltpu.VMEM)
+    vmem = pl.BlockSpec(memory_space=out_space)
     return pl.pallas_call(
         kernel,
         out_shape=outs,
@@ -172,6 +172,12 @@
         out_ref[i] = merged
 
 
+def write_out(value_ref, out_ref, sem):
+    copy = pltpu.make_async_copy(value_ref, out_ref, sem)
+    copy.start()
+    copy.wait()
+
+
 def mix(merged_ref, w_ref, kept_ref, given_ref):
     mixed = jnp.dot(
         all_rows(merged_ref).astype(BF16), w_ref[...], preferred_element_type=F32
@@ -306,11 +312,18 @@
         exchanged(merged, "kv"),
         output_weight,
     )
+    swapped = lax.ppermute(given, "tp", swap)
+    new_state, _ = lax.optimization_barrier((new_state, given))
+    new_state = local_call(
+        write_out,
+        jax.ShapeDtypeStruct(retention_state.shape, F32),
+        new_state,
+        scratch=(pltpu.SemaphoreType.DMA,),
+        out_space=pl.ANY,
+    )
+    swapped, new_state = lax.optimization_barrier((swapped, new_state))
     chip_sum = local_call(
-        add_given,
-        shaped((members // 2, batch, half), BF16),
-        kept,
-        lax.ppermute(given, "tp", swap),
+        add_given, shaped((members // 2, batch, half), BF16), kept, swapped
     )
     residual_half = local_call(
         add_chips,

time: 103 us -> 102 us (level)
  blocking collectives: 79 us -> 91.8 us
  waiting for transfers between devices: 8.57 us -> 0.86 us
  starting transfers between devices: 9.2 us -> 3.31 us
    all_to_all x6 -> x7, blocking collectives: 79 us -> 91.8 us  [exchanged(): lax.all_to_all(blocks, axis, 0, 0, tiled=True, axis_index_groups=groups)]
    all_to_all x1 -> x0, waiting for transfers between devices: 6.85 us -> none  [exchanged(): lax.all_to_all(blocks, axis, 0, 0, tiled=True, axis_index_groups=groups)]
    all_to_all x1 -> x0, starting transfers between devices: 5.87 us -> none  [exchanged(): lax.all_to_all(blocks, axis, 0, 0, tiled=True, axis_index_groups=groups)]
    pallas_call x10 -> x11, Pallas kernels: 4.22 us -> 4.58 us  [local_call(): pl.pallas_call(kernel, out_shape=outs, in_specs=[pl.BlockSpec(memory_spac...]
  transfers between devices with their start and end apart: 3 -> 2, of which waited for: 3 -> 1; matrix products, arithmetic and copies ran while one was open for 1% -> 0% of each run, Pallas kernels for 0% -> 1%
where the time goes in v2:
time: 102 us; the launch traced here: 101 us
  blocking collectives  91.8 us (90%)
  Pallas kernels  4.58 us (4%)
  starting transfers between devices  3.31 us (3%)
    all_to_all x7, blocking collectives, exchanged(): lax.all_to_all(blocks, axis, 0, 0, tiled=True, axis_index_groups=groups)  91.8 us
    pallas_call x11, Pallas kernels, local_call(): pl.pallas_call(kernel, out_shape=outs, in_specs=[pl.BlockSpec(memory_spac...  4.58 us
    ppermute x1, starting transfers between devices, on_device(): swapped = lax.ppermute(given, 'tp', swap)  2.76 us
  transfers between devices with their start and end apart: 2, of which 1 were waited for; matrix products, arithmetic and copies ran while one was open for 0% of the time, Pallas kernels for 1%

profile of v2, /device:TPU:1, one launch (start us, length us, event | category | flops | bytes accessed | tf_op | source)
XLA Modules:
  0.0 101.4 jit_solution(4873367911822149957)
XLA Ops:
  0.6 1.2 %shard_map.140 = (bf16[16,16,128]{2,1,0:T(8,128)(2,1)S(1)}, f32[8,128]{1,0:T(8,128)S(1)}, f32[8,128]{1,0:T(8,128)S(1)}, f32[256]{0:T(256)S(1)}, f32[256]{0:T(256...) custom-call(bf16[16,128]{1,0:T(8,128)(2,1)} %bitcast.6, ...), custom_call_target="tpu_custom_call" | custom-call | tf_op jit(solution)/shard_map/pallas_call | solution.py:25
  1.8 0.0 copy-start
  1.8 17.7 %all_to_all.35.x_ref = bf16[16,16,128]{2,1,0:T(8,128)(2,1)S(1)} all-to-all(bf16[16,16,128]{2,1,0:T(8,128)(2,1)S(1)} %get-tuple-element.22), channel_id=1, replica_groups=mesh['kv'=16,'tp'=16] {'tp'}, dimensions={0} | all-to-all | bytes 131072 | tf_op jit(solution)/shard_map/all_to_all | solution.py:243
  19.5 0.3 shard_map.141
  19.8 14.6 %all_to_all.36.parts_ref = bf16[16,8,896]{2,1,0:T(8,128)(2,1)S(1)} all-to-all(bf16[16,8,896]{2,1,0:T(8,128)(2,1)S(1)} %get-tuple-element.28), channel_id=1, replica_groups=mesh['kv'=16,'tp'=16] {'kv'}, dimensions={0} | all-to-all | bytes 458752 | tf_op jit(solution)/shard_map/all_to_all | solution.py:243
  34.3 0.0 copy-done
  34.4 0.5 shard_map.142
  34.9 0.0 copy-start.4
  34.9 9.3 %all_to_all.37.merged_ref = bf16[16,8,256]{2,1,0:T(8,128)(2,1)S(1)} all-to-all(bf16[16,8,256]{2,1,0:T(8,128)(2,1)S(1)} %get-tuple-element.31), channel_id=1, replica_groups=mesh['kv'=16,'tp'=16] {'kv'}, dimensions={0} | all-to-all | bytes 131072 | tf_op jit(solution)/shard_map/all_to_all | solution.py:243
  44.2 0.0 copy-done.4
  44.2 0.2 shard_map.143
  44.4 2.8 %collective-permute-start = (bf16[128,128]{1,0:T(8,128)(2,1)S(1)}, bf16[128,128]{1,0:T(8,128)(2,1)S(1)}, u32[]{:S(2)}, u32[]{:S(2)}) collective-permute-start(bf16[128,128]{1,0:T(8,128)(2,1)S(1)} %get-tuple-element.33), channel_id=1, source_target_pairs={{0,1},{1,0},{2,3},{3,2},{4,5},{5,4},{6,7},{7,6},{8,9},{9,8},{10,11... | collective-permute-start | bytes 98312 | tf_op jit(solution)/shard_map/ppermute | solution.py:315
  47.2 1.0 shard_map.144
  48.1 0.0 collective-permute-done.given_ref
  48.2 0.0 copy-start.1
  48.2 0.0 copy-start.2
  48.2 14.9 %all_to_all.38.parts_ref = bf16[8,128,128]{2,1,0:T(8,128)(2,1)S(1)} all-to-all(bf16[8,128,128]{2,1,0:T(8,128)(2,1)S(1)} %shard_map.145), channel_id=1, replica_groups={{0,2,4,6,8,10,12,14},{1,3,5,7,9,11,13,15},{16,18,20,22,24,26,28,30},{17..., dimensions={0} | all-to-all | bytes 524288 | tf_op jit(solution)/shard_map/all_to_all | solution.py:243
  63.2 0.5 collective-permute-start.1
  63.7 0.9 collective-permute-done.1.other_ref
  64.6 0.0 copy-done.1
  64.6 0.0 copy-done.2
  64.6 0.4 shard_map.147
  65.0 12.4 %all_to_all.39.parts_ref = bf16[16,8,1536]{2,1,0:T(8,128)(2,1)S(1)} all-to-all(bf16[16,8,1536]{2,1,0:T(8,128)(2,1)S(1)} %get-tuple-element.39), channel_id=1, replica_groups=mesh['kv'=16,'tp'=16] {'kv'}, dimensions={0} | all-to-all | bytes 786432 | tf_op jit(solution)/shard_map/all_to_all | solution.py:243
  77.4 0.0 copy-start.3
  77.4 0.1 shard_map.148
  77.5 10.1 %all_to_all.40.hidden_ref = bf16[16,8,704]{2,1,0:T(8,128)(2,1)S(1)} all-to-all(bf16[16,8,704]{2,1,0:T(8,128)(2,1)S(1)} %shard_map.148), channel_id=1, replica_groups=mesh['kv'=16,'tp'=16] {'kv'}, dimensions={0} | all-to-all | bytes 360448 | tf_op jit(solution)/shard_map/all_to_all | solution.py:243
  87.6 0.0 copy-done.3
  87.6 0.3 shard_map.149
  87.9 12.8 %all_to_all.41.parts_ref = bf16[16,16,128]{2,1,0:T(8,128)(2,1)S(1)} all-to-all(bf16[16,16,128]{2,1,0:T(8,128)(2,1)S(1)} %shard_map.149), channel_id=1, replica_groups=mesh['kv'=16,'tp'=16] {'tp'}, dimensions={0} | all-to-all | bytes 131072 | tf_op jit(solution)/shard_map/all_to_all | solution.py:243
  100.8 0.6 shard_map.150
  (2 shorter events, 0.1 us)
Async XLA Ops:
  1.8 32.6 %copy-start = (f32[8,1,128,256]{3,2,1,0:T(8,128)S(1)}, f32[8,1,128,256]{3,2,1,0:T(8,128)}, u32[]{:S(2)}) copy-start(f32[8,1,128,256]{3,2,1,0:T(8,128)} %state_ref.1) | copy-start | bytes 3145732
  34.9 9.3 %copy-start.4 = (bf16[256,256]{1,0:T(8,128)(2,1)S(1)}, bf16[256,256]{1,0:T(8,128)(2,1)}, u32[]{:S(2)}) copy-start(bf16[256,256]{1,0:T(8,128)(2,1)} %w_ref.2) | copy-start | bytes 393220
  44.4 3.8 %collective-permute-start = (bf16[128,128]{1,0:T(8,128)(2,1)S(1)}, bf16[128,128]{1,0:T(8,128)(2,1)S(1)}, u32[]{:S(2)}, u32[]{:S(2)}) collective-permute-start(bf16[128,128]{1,0:T(8,128)(2,1)S(1)} %get-tuple-element.33), channel_id=1, source_target_pairs={{0,1},{1,0},{2,3},{3,2},{4,5},{5,4},{6,7},{7,6},{8,9},{9,8},{10,11... | collective-permute-start | bytes 98312 | tf_op jit(solution)/shard_map/ppermute | solution.py:315
  48.2 16.4 %copy-start.1 = (bf16[256,704]{0,1:T(8,128)(2,1)S(1)}, bf16[256,704]{0,1:T(8,128)(2,1)}, u32[]{:S(2)}) copy-start(bf16[256,704]{0,1:T(8,128)(2,1)} %param.23) | copy-start | bytes 1081348
  48.2 16.4 %copy-start.2 = (bf16[256,704]{0,1:T(8,128)(2,1)S(1)}, bf16[256,704]{0,1:T(8,128)(2,1)}, u32[]{:S(2)}) copy-start(bf16[256,704]{0,1:T(8,128)(2,1)} %param.24) | copy-start | bytes 1081348
  63.2 1.4 %collective-permute-start.1 = (bf16[128,128]{1,0:T(8,128)(2,1)S(1)}, bf16[128,128]{1,0:T(8,128)(2,1)S(1)}, u32[]{:S(2)}, u32[]{:S(2)}) collective-permute-start(bf16[128,128]{1,0:T(8,128)(2,1)S(1)} %shard_map.146.half_ref), channel_id=1, source_target_pairs={{0,1},{1,0},{2,3},{3,2},{4,5},{5,4},{6,7},{7,6},{8,9},{9,8},{10,11... | collective-permute-start | bytes 98312 | tf_op jit(solution)/shard_map/ppermute | solution.py:338
  77.4 10.3 %copy-start.3 = (bf16[704,256]{1,0:T(8,128)(2,1)S(1)}, bf16[704,256]{1,0:T(8,128)(2,1)}, u32[]{:S(2)}) copy-start(bf16[704,256]{1,0:T(8,128)(2,1)} %w_ref.3) | copy-start | bytes 1081348

commit v3 on v2

--- a/solution.py
+++ b/solution.py
@@ -5,7 +5,7 @@
 from jax import lax
 from jax.experimental import pallas as pl
 from jax.experimental.pallas import tpu as pltpu
-from jax.sharding import PartitionSpec as P
+from jax.sharding import Mesh, PartitionSpec as P
 
 D = 4096
 HEADS = 16
@@ -30,6 +30,10 @@
         scratch_shapes=scratch,
         compiler_params=pltpu.CompilerParams(vmem_limit_bytes=limit),
     )(*operands)
+
+
+def tp_index():
+    return lax.axis_index("z") * lax.axis_size("core") + lax.axis_index("core")
 
 
 def shaped(shape, dtype):
@@ -98,7 +102,7 @@
         at += w_ref.shape[1]
     squares = jnp.sum(x * x, axis=1, keepdims=True)
     store_rows(out_ref, jnp.broadcast_to(squares, (x.shape[0], LANES)), at)
-    core = lax.rem(lax.axis_index("tp"), 2)
+    core = lax.axis_index("core")
     width = half_ref.shape[1]
     half_ref[...] = jnp.where(core == 0, x[:, :width], x[:, width:]).astype(BF16)
 
@@ -155,7 +159,7 @@
     value = (sums[:, 2 * QK : 2 * QK + VD] * wide_scale).astype(BF16).astype(F32)
     gate = sums[:, 2 * QK + VD : 2 * QK + 2 * VD] * wide_scale
     columns = jnp.concatenate([query, key] * (QK // (2 * rows)), axis=0).T
-    head = jnp.full((1, VD), lax.axis_index("tp"), jnp.int32).astype(F32)
+    head = jnp.full((1, VD), tp_index(), jnp.int32).astype(F32)
     decay = 1.0 - jnp.exp2(-5.0 - 10.0 * head / (HEADS - 1))
     retained = []
     for i in range(rows):
@@ -178,19 +182,18 @@
     copy.wait()
 
 
-def mix(merged_ref, w_ref, kept_ref, given_ref):
-    mixed = jnp.dot(
-        all_rows(merged_ref).astype(BF16), w_ref[...], preferred_element_type=F32
-    )
-    width = kept_ref.shape[1]
-    low, high = mixed[:, :width], mixed[:, width:]
-    first = lax.rem(lax.axis_index("tp"), 2) == 0
-    kept_ref[...] = jnp.where(first, low, high)
-    given_ref[...] = jnp.where(first, high, low).astype(BF16)
-
-
-def add_given(kept_ref, given_ref, out_ref):
-    total = (kept_ref[...] + given_ref[...].astype(F32)).astype(BF16)
+def mix(merged_ref, own_ref, other_ref, out_ref):
+    core = lax.axis_index("core")
+    half = out_ref.shape[2]
+    total = None
+    for w_ref, which in ((own_ref, core), (other_ref, 1 - core)):
+        merged = jnp.concatenate(
+            [merged_ref[i + which].astype(F32) for i in range(0, merged_ref.shape[0], 2)], axis=0
+        )
+        weight = jnp.where(core == 0, w_ref[:, :half], w_ref[:, half:])
+        part = jnp.dot(merged.astype(BF16), weight, preferred_element_type=F32)
+        total = part if total is None else total + part
+    total = total.astype(BF16)
     for i in range(out_ref.shape[0]):
         out_ref[i] = total
 
@@ -200,8 +203,8 @@
 
 
 def expand(half_ref, other_ref, gain_ref, gate_ref, up_ref, out_ref, mine_ref, flipped_ref):
-    me = lax.axis_index("tp")
-    first = lax.rem(me, 2) == 0
+    me = tp_index()
+    first = lax.axis_index("core") == 0
     half, other = half_ref[...].astype(F32), other_ref[...].astype(F32)
     x = jnp.concatenate(
         [jnp.where(first, half, other), jnp.where(first, other, half)], axis=1
@@ -258,15 +261,16 @@
     ffn_up,
     ffn_down,
 ):
-    owners, members = lax.axis_size("kv"), lax.axis_size("tp")
+    owners, chips, cores = (lax.axis_size(a) for a in ("kv", "z", "core"))
+    members = chips * cores
     batch, own_width = tokens.shape
     rows = batch // owners
     block = own_width * members
     half = block // 2
     units = ffn_gate.shape[1]
     middle = -(-(units + 1) // LANES) * LANES
-    swap = [(i, i ^ 1) for i in range(members)]
-    along_z = [[i + c for i in range(0, members, 2)] for c in range(2)]
+    swap = [(0, 1), (1, 0)]
+    along_z = [[3 * i % chips for i in range(chips)]]
 
     weights = (query_weight, key_weight, value_weight, gate_weight)
     fetch = (mixer_gain, channel_gain, *weights)
@@ -289,7 +293,9 @@
         space=pltpu.HBM,
         limit=FULL_VMEM_BYTES,
     )
-    features = exchanged(copies, "tp")
+    other_weight = lax.ppermute(output_weight, "core", swap)
+    features = exchanged(copies, ("z", "core"))
+    features, other_weight = lax.optimization_barrier((features, other_weight))
     width = 2 * QK + 2 * VD + LANES
     parts, token_half = local_call(
         project,
@@ -300,20 +306,27 @@
     )
     merged, new_state = local_call(
         retain,
-        (shaped((owners, rows, VD), BF16), shaped(retention_state.shape, F32)),
+        (shaped((owners * cores, rows, VD), BF16), shaped(retention_state.shape, F32)),
         exchanged(parts, "kv"),
         sine,
         cosine,
         retention_state,
     )
-    kept, given = local_call(
+    chip_sum = local_call(
         mix,
-        (shaped((batch, half), F32), shaped((batch, half), BF16)),
-        exchanged(merged, "kv"),
+        shaped((chips, batch, half), BF16),
+        exchanged(merged, ("kv", "core")),
         output_weight,
-    )
-    swapped = lax.ppermute(given, "tp", swap)
-    new_state, _ = lax.optimization_barrier((new_state, given))
+        other_weight,
+    )
+    residual_half = local_call(
+        add_chips,
+        shaped((batch, half), BF16),
+        exchanged(chip_sum, "z", along_z),
+        token_half,
+    )
+    residual_other = lax.ppermute(residual_half, "core", swap)
+    new_state, _ = lax.optimization_barrier((new_state, residual_half))
     new_state = local_call(
         write_out,
         jax.ShapeDtypeStruct(retention_state.shape, F32),
@@ -321,21 +334,12 @@
         scratch=(pltpu.SemaphoreType.DMA,),
         out_space=pl.ANY,
     )
-    swapped, new_state = lax.optimization_barrier((swapped, new_state))
-    chip_sum = local_call(
-        add_given, shaped((members // 2, batch, half), BF16), kept, swapped
-    )
-    residual_half = local_call(
-        add_chips,
-        shaped((batch, half), BF16),
-        exchanged(chip_sum, "tp", along_z),
-        token_half,
-    )
+    residual_other, new_state = lax.optimization_barrier((residual_other, new_state))
     parts, mine = local_call(
         expand,
         (shaped((owners, rows, 2 * middle), BF16), shaped((own_width, batch), F32)),
         residual_half,
-        lax.ppermute(residual_half, "tp", swap),
+        residual_other,
         channel_gain,
         ffn_gate.T,
         ffn_up.T,
@@ -351,28 +355,32 @@
         ffn_down,
     )
     layer_output = local_call(
-        finish, jax.ShapeDtypeStruct((own_width, batch), BF16), exchanged(down, "tp"), mine
+        finish, jax.ShapeDtypeStruct((own_width, batch), BF16), exchanged(down, ("z", "core")), mine
     )
     return (layer_output.T, new_state)
 
 
 def solution(mesh):
+    split = Mesh(
+        mesh.devices.reshape(mesh.shape["kv"], mesh.shape["tp"] // 2, 2), ("kv", "z", "core")
+    )
+    tp = ("z", "core")
     in_specs = (
-        P(None, ("kv", "tp")),
+        P(None, ("kv", *tp)),
         P("kv"),
-        P("kv", "tp", None, None),
+        P("kv", tp, None, None),
         P("kv"),
-        P("kv", "tp"),
-        P("kv", "tp"),
-        P("kv", "tp"),
-        P("kv", "tp"),
-        P("tp", "kv"),
+        P("kv", tp),
+        P("kv", tp),
+        P("kv", tp),
+        P("kv", tp),
+        P(tp, "kv"),
         P("kv"),
-        P("kv", "tp"),
-        P("kv", "tp"),
-        P("tp", "kv"),
-    )
-    out_specs = (P(None, ("kv", "tp")), P("kv", "tp", None, None))
+        P("kv", tp),
+        P("kv", tp),
+        P(tp, "kv"),
+    )
+    out_specs = (P(None, ("kv", *tp)), P("kv", tp, None, None))
     return jax.shard_map(
-        on_device, mesh=mesh, in_specs=in_specs, out_specs=out_specs, check_vma=False
-    )
+        on_device, mesh=split, in_specs=in_specs, out_specs=out_specs, check_vma=False
+    )

time: 102 us -> 101 us (level)
  blocking collectives: 91.8 us -> 89.3 us
  starting transfers between devices: 3.31 us -> 5.08 us
    all_to_all x7, blocking collectives: 91.8 us -> 89.3 us  [exchanged(): lax.all_to_all(blocks, axis, 0, 0, tiled=True, axis_index_groups=groups)]
    ppermute x2, starting transfers between devices: 3.31 us -> 5.08 us  [the longest x1 3.29 us: on_device(): other_weight = lax.ppermute(output_weight, 'core', swap)]
    pallas_call x11 -> x10, Pallas kernels: 4.58 us -> 4.58 us  [local_call(): pl.pallas_call(kernel, out_shape=outs, in_specs=[pl.BlockSpec(memory_spac...]
  transfers between devices with their start and end apart: 2 -> 2, of which waited for: 1 -> 0; matrix products, arithmetic and copies ran while one was open for 0% -> 0% of each run, Pallas kernels for 1% -> 2%
where the time goes in v3:
time: 101 us; the launch traced here: 100 us
  blocking collectives  89.3 us (88%)
  starting transfers between devices  5.08 us (5%)
  Pallas kernels  4.58 us (5%)
    all_to_all x7, blocking collectives, exchanged(): lax.all_to_all(blocks, axis, 0, 0, tiled=True, axis_index_groups=groups)  89.3 us
    pallas_call x10, Pallas kernels, local_call(): pl.pallas_call(kernel, out_shape=outs, in_specs=[pl.BlockSpec(memory_spac...  4.58 us
    ppermute x1, starting transfers between devices, on_device(): other_weight = lax.ppermute(output_weight, 'core', swap)  3.29 us
  transfers between devices with their start and end apart: 2, of which 0 were waited for; matrix products, arithmetic and copies ran while one was open for 0% of the time, Pallas kernels for 2%

profile of v3, /device:TPU:1, one launch (start us, length us, event | category | flops | bytes accessed | tf_op | source)
XLA Modules:
  0.0 100.2 jit_solution(14998614773753247769)
XLA Ops:
  0.6 3.3 %collective-permute-start = (bf16[256,256]{1,0:T(8,128)(2,1)}, bf16[256,256]{1,0:T(8,128)(2,1)S(1)}, u32[]{:S(2)}, u32[]{:S(2)}) collective-permute-start(bf16[256,256]{1,0:T(8,128)(2,1)} %own_ref.1), channel_id=1, source_target_pairs={{0,1},{1,0},{2,3},{3,2},{4,5},{5,4},{6,7},{7,6},{8,9},{9,8},{10,11... | collective-permute-start | bytes 393224 | tf_op jit(solution)/shard_map/ppermute | solution.py:296
  3.9 1.1 %shard_map.140 = (bf16[16,16,128]{2,1,0:T(8,128)(2,1)S(1)}, f32[8,128]{1,0:T(8,128)S(1)}, f32[8,128]{1,0:T(8,128)S(1)}, f32[256]{0:T(256)S(1)}, f32[256]{0:T(256...) custom-call(bf16[16,128]{1,0:T(8,128)(2,1)} %bitcast.6, ...), custom_call_target="tpu_custom_call" | custom-call | tf_op jit(solution)/shard_map/pallas_call | solution.py:25
  5.1 0.0 copy-start
  5.1 14.6 %all_to_all.35.x_ref = bf16[16,16,128]{2,1,0:T(8,128)(2,1)S(1)} all-to-all(bf16[16,16,128]{2,1,0:T(8,128)(2,1)S(1)} %get-tuple-element.22), channel_id=1, replica_groups=mesh['kv'=16,'z'=8,'core'=2] {'z','core'}, dimensions={0} | all-to-all | bytes 131072 | tf_op jit(solution)/shard_map/all_to_all | solution.py:246
  19.7 0.0 collective-permute-done.other_ref
  19.7 0.3 shard_map.141
  20.0 14.6 %all_to_all.36.parts_ref = bf16[16,8,896]{2,1,0:T(8,128)(2,1)S(1)} all-to-all(bf16[16,8,896]{2,1,0:T(8,128)(2,1)S(1)} %get-tuple-element.29), channel_id=1, replica_groups=mesh['kv'=16,'z'=8,'core'=2] {'kv'}, dimensions={0} | all-to-all | bytes 458752 | tf_op jit(solution)/shard_map/all_to_all | solution.py:246
  34.5 0.0 copy-done
  34.5 0.6 shard_map.142
  35.1 0.0 copy-start.4
  35.1 12.0 %all_to_all.37.merged_ref = bf16[32,8,256]{2,1,0:T(8,128)(2,1)S(1)} all-to-all(bf16[32,8,256]{2,1,0:T(8,128)(2,1)S(1)} %get-tuple-element.32), channel_id=1, replica_groups=mesh['kv'=16,'z'=8,'core'=2] {'kv','core'}, dimensions={0} | all-to-all | bytes 262144 | tf_op jit(solution)/shard_map/all_to_all | solution.py:246
  47.1 0.0 copy-done.4
  47.1 0.2 shard_map.143
  47.3 12.8 %all_to_all.38.parts_ref = bf16[8,128,128]{2,1,0:T(8,128)(2,1)S(1)} all-to-all(bf16[8,128,128]{2,1,0:T(8,128)(2,1)S(1)} %shard_map.143), channel_id=1, replica_groups={{0,6,12,2,8,14,4,10},{1,7,13,3,9,15,5,11},{16,22,28,18,24,30,20,26},{17..., dimensions={0} | all-to-all | bytes 524288 | tf_op jit(solution)/shard_map/all_to_all | solution.py:246
  60.2 1.8 %collective-permute-start.1 = (bf16[128,128]{1,0:T(8,128)(2,1)S(1)}, bf16[128,128]{1,0:T(8,128)(2,1)S(1)}, u32[]{:S(2)}, u32[]{:S(2)}) collective-permute-start(bf16[128,128]{1,0:T(8,128)(2,1)S(1)} %shard_map.144.half_ref), channel_id=1, source_target_pairs={{0,1},{1,0},{2,3},{3,2},{4,5},{5,4},{6,7},{7,6},{8,9},{9,8},{10,11... | collective-permute-start | bytes 98312 | tf_op jit(solution)/shard_map/ppermute | solution.py:328
  62.0 0.0 copy-start.1
  62.0 0.0 copy-start.2
  62.0 1.0 shard_map.145
  63.0 0.0 collective-permute-done.1.other_ref
  63.0 0.2 copy-done.1
  63.2 0.3 copy-done.2
  63.4 0.4 shard_map.146
  63.8 12.4 %all_to_all.39.parts_ref = bf16[16,8,1536]{2,1,0:T(8,128)(2,1)S(1)} all-to-all(bf16[16,8,1536]{2,1,0:T(8,128)(2,1)S(1)} %get-tuple-element.39), channel_id=1, replica_groups=mesh['kv'=16,'z'=8,'core'=2] {'kv'}, dimensions={0} | all-to-all | bytes 786432 | tf_op jit(solution)/shard_map/all_to_all | solution.py:246
  76.2 0.0 copy-start.3
  76.2 0.1 shard_map.147
  76.3 10.3 %all_to_all.40.hidden_ref = bf16[16,8,704]{2,1,0:T(8,128)(2,1)S(1)} all-to-all(bf16[16,8,704]{2,1,0:T(8,128)(2,1)S(1)} %shard_map.147), channel_id=1, replica_groups=mesh['kv'=16,'z'=8,'core'=2] {'kv'}, dimensions={0} | all-to-all | bytes 360448 | tf_op jit(solution)/shard_map/all_to_all | solution.py:246
  86.6 0.0 copy-done.3
  86.6 0.3 shard_map.148
  86.9 12.6 %all_to_all.41.parts_ref = bf16[16,16,128]{2,1,0:T(8,128)(2,1)S(1)} all-to-all(bf16[16,16,128]{2,1,0:T(8,128)(2,1)S(1)} %shard_map.148), channel_id=1, replica_groups=mesh['kv'=16,'z'=8,'core'=2] {'z','core'}, dimensions={0} | all-to-all | bytes 131072 | tf_op jit(solution)/shard_map/all_to_all | solution.py:246
  99.5 0.6 shard_map.149
  (1 shorter events, 0.0 us)
Async XLA Ops:
  0.6 19.0 %collective-permute-start = (bf16[256,256]{1,0:T(8,128)(2,1)}, bf16[256,256]{1,0:T(8,128)(2,1)S(1)}, u32[]{:S(2)}, u32[]{:S(2)}) collective-permute-start(bf16[256,256]{1,0:T(8,128)(2,1)} %own_ref.1), channel_id=1, source_target_pairs={{0,1},{1,0},{2,3},{3,2},{4,5},{5,4},{6,7},{7,6},{8,9},{9,8},{10,11... | collective-permute-start | bytes 393224 | tf_op jit(solution)/shard_map/ppermute | solution.py:296
  5.1 29.5 %copy-start = (f32[8,1,128,256]{3,2,1,0:T(8,128)S(1)}, f32[8,1,128,256]{3,2,1,0:T(8,128)}, u32[]{:S(2)}) copy-start(f32[8,1,128,256]{3,2,1,0:T(8,128)} %state_ref.1) | copy-start | bytes 3145732
  35.1 12.0 %copy-start.4 = (bf16[256,256]{1,0:T(8,128)(2,1)S(1)}, bf16[256,256]{1,0:T(8,128)(2,1)}, u32[]{:S(2)}) copy-start(bf16[256,256]{1,0:T(8,128)(2,1)} %own_ref.1) | copy-start | bytes 393220
  60.2 2.8 %collective-permute-start.1 = (bf16[128,128]{1,0:T(8,128)(2,1)S(1)}, bf16[128,128]{1,0:T(8,128)(2,1)S(1)}, u32[]{:S(2)}, u32[]{:S(2)}) collective-permute-start(bf16[128,128]{1,0:T(8,128)(2,1)S(1)} %shard_map.144.half_ref), channel_id=1, source_target_pairs={{0,1},{1,0},{2,3},{3,2},{4,5},{5,4},{6,7},{7,6},{8,9},{9,8},{10,11... | collective-permute-start | bytes 98312 | tf_op jit(solution)/shard_map/ppermute | solution.py:328
  62.0 1.2 %copy-start.1 = (bf16[256,704]{0,1:T(8,128)(2,1)S(1)}, bf16[256,704]{0,1:T(8,128)(2,1)}, u32[]{:S(2)}) copy-start(bf16[256,704]{0,1:T(8,128)(2,1)} %param.23) | copy-start | bytes 1081348
  62.0 1.5 %copy-start.2 = (bf16[256,704]{0,1:T(8,128)(2,1)S(1)}, bf16[256,704]{0,1:T(8,128)(2,1)}, u32[]{:S(2)}) copy-start(bf16[256,704]{0,1:T(8,128)(2,1)} %param.24) | copy-start | bytes 1081348
  76.2 10.4 %copy-start.3 = (bf16[704,256]{1,0:T(8,128)(2,1)S(1)}, bf16[704,256]{1,0:T(8,128)(2,1)}, u32[]{:S(2)}) copy-start(bf16[704,256]{1,0:T(8,128)(2,1)} %w_ref.1) | copy-start | bytes 1081348

commit v4 on v3

--- a/solution.py
+++ b/solution.py
@@ -12,6 +12,7 @@
 QK = 128
 VD = 256
 LANES = 128
+KV_ORDER = (0, 8, 15, 14, 5, 2, 3, 11, 6, 13, 10, 4, 9, 7, 1, 12)
 F32 = jnp.float32
 BF16 = jnp.bfloat16
 VMEM_BYTES = 8 << 20
@@ -40,16 +41,23 @@
     return pltpu.VMEM(shape, dtype)
 
 
+def kv_order(owners):
+    return KV_ORDER if owners == len(KV_ORDER) else tuple(range(owners))
+
+
 def store_rows(out_ref, value, start):
     each = out_ref.shape[1]
-    for owner in range(out_ref.shape[0]):
-        out_ref[owner, :, start : start + value.shape[1]] = value[
+    for at, owner in enumerate(kv_order(out_ref.shape[0])):
+        out_ref[at, :, start : start + value.shape[1]] = value[
             owner * each : (owner + 1) * each
         ].astype(out_ref.dtype)
 
 
 def all_rows(ref):
-    return jnp.concatenate([ref[i].astype(F32) for i in range(ref.shape[0])], axis=0)
+    order = kv_order(ref.shape[0])
+    return jnp.concatenate(
+        [ref[order.index(owner)].astype(F32) for owner in range(ref.shape[0])], axis=0
+    )
 
 
 def summed(ref):
@@ -198,11 +206,12 @@
         out_ref[i] = total
 
 
-def add_chips(parts_ref, token_ref, out_ref):
+def add_chips(parts_ref, token_ref, *refs):
+    out_ref = refs[-1]
     out_ref[...] = (token_ref[...].astype(F32) + summed(parts_ref)).astype(BF16)
 
 
-def expand(half_ref, other_ref, gain_ref, gate_ref, up_ref, out_ref, mine_ref, flipped_ref):
+def expand(half_ref, other_ref, gain_ref, gate_ref, up_ref, out_ref, mine_ref):
     me = tp_index()
     first = lax.axis_index("core") == 0
     half, other = half_ref[...].astype(F32), other_ref[...].astype(F32)
@@ -217,9 +226,12 @@
     spare = out_ref.shape[2] // 2 - units
     squares = jnp.broadcast_to(jnp.sum(x * x, axis=1, keepdims=True), (x.shape[0], spare))
     store_rows(out_ref, jnp.concatenate([gate, squares, up, squares], axis=1), 0)
-    flipped_ref[...] = x.T
-    width = mine_ref.shape[0]
-    mine_ref[...] = flipped_ref[pl.ds(pl.multiple_of(me * width, width), width), :]
+    shape = (mine_ref.shape[0], x.shape[1])
+    row = lax.broadcasted_iota(jnp.int32, shape, 0)
+    pick = lax.broadcasted_iota(jnp.int32, shape, 1) == row + me * shape[0]
+    mine_ref[...] = lax.dot_general(
+        pick.astype(BF16), x.astype(BF16), contract, preferred_element_type=F32
+    )
 
 
 def activate(parts_ref, out_ref):
@@ -265,12 +277,13 @@
     members = chips * cores
     batch, own_width = tokens.shape
     rows = batch // owners
-    block = own_width * members
-    half = block // 2
+    half = own_width * members // cores
     units = ffn_gate.shape[1]
     middle = -(-(units + 1) // LANES) * LANES
     swap = [(0, 1), (1, 0)]
-    along_z = [[3 * i % chips for i in range(chips)]]
+    gate_rows, up_rows = ffn_gate.T, ffn_up.T
+    along_z = [[0, 1, 4, 3, 2, 5, 7, 6]] if chips == 8 else None
+    along_kv = [list(kv_order(owners))]
 
     weights = (query_weight, key_weight, value_weight, gate_weight)
     fetch = (mixer_gain, channel_gain, *weights)
@@ -307,7 +320,7 @@
     merged, new_state = local_call(
         retain,
         (shaped((owners * cores, rows, VD), BF16), shaped(retention_state.shape, F32)),
-        exchanged(parts, "kv"),
+        exchanged(parts, "kv", along_kv),
         sine,
         cosine,
         retention_state,
@@ -324,6 +337,8 @@
         shaped((batch, half), BF16),
         exchanged(chip_sum, "z", along_z),
         token_half,
+        gate_rows,
+        up_rows,
     )
     residual_other = lax.ppermute(residual_half, "core", swap)
     new_state, _ = lax.optimization_barrier((new_state, residual_half))
@@ -341,17 +356,16 @@
         residual_half,
         residual_other,
         channel_gain,
-        ffn_gate.T,
-        ffn_up.T,
-        scratch=(pltpu.VMEM((block, batch), F32),),
+        gate_rows,
+        up_rows,
     )
     hidden = local_call(
-        activate, shaped((owners, rows, units), BF16), exchanged(parts, "kv")
+        activate, shaped((owners, rows, units), BF16), exchanged(parts, "kv", along_kv)
     )
     down = local_call(
         contract_units,
         shaped((members, own_width, batch), BF16),
-        exchanged(hidden, "kv"),
+        exchanged(hidden, "kv", along_kv),
         ffn_down,
     )
     layer_output = local_call(

time: 101 us -> 99.8 us (0.988)
  blocking collectives: 89.3 us -> 87.6 us
  starting transfers between devices: 5.08 us -> 6.42 us
    all_to_all x7, blocking collectives: 89.3 us -> 87.6 us  [exchanged(): lax.all_to_all(blocks, axis, 0, 0, tiled=True, axis_index_groups=groups)]
    ppermute x1, starting transfers between devices: 1.79 us -> 3.14 us  [on_device(): residual_other = lax.ppermute(residual_half, 'core', swap)]
where the time goes in v4:
time: 99.8 us; the launch traced here: 99.4 us
  blocking collectives  87.6 us (88%)
  starting transfers between devices  6.42 us (6%)
  Pallas kernels  4.58 us (5%)
    all_to_all x7, blocking collectives, exchanged(): lax.all_to_all(blocks, axis, 0, 0, tiled=True, axis_index_groups=groups)  87.6 us
    pallas_call x10, Pallas kernels, local_call(): pl.pallas_call(kernel, out_shape=outs, in_specs=[pl.BlockSpec(memory_spac...  4.58 us
    ppermute x1, starting transfers between devices, on_device(): other_weight = lax.ppermute(output_weight, 'core', swap)  3.29 us
    ppermute x1, starting transfers between devices, on_device(): residual_other = lax.ppermute(residual_half, 'core', swap)  3.14 us
  transfers between devices with their start and end apart: 2, of which 0 were waited for; matrix products, arithmetic and copies ran while one was open for 0% of the time, Pallas kernels for 2%

profile of v4, /device:TPU:1, one launch (start us, length us, event | category | flops | bytes accessed | tf_op | source)
XLA Modules:
  0.0 99.4 jit_solution(795468114022751111)
XLA Ops:
  0.6 3.3 %collective-permute-start = (bf16[256,256]{1,0:T(8,128)(2,1)}, bf16[256,256]{1,0:T(8,128)(2,1)S(1)}, u32[]{:S(2)}, u32[]{:S(2)}) collective-permute-start(bf16[256,256]{1,0:T(8,128)(2,1)} %own_ref.1), channel_id=1, source_target_pairs={{0,1},{1,0},{2,3},{3,2},{4,5},{5,4},{6,7},{7,6},{8,9},{9,8},{10,11... | collective-permute-start | bytes 393224 | tf_op jit(solution)/shard_map/ppermute | solution.py:309
  3.9 1.1 %shard_map.140 = (bf16[16,16,128]{2,1,0:T(8,128)(2,1)S(1)}, f32[8,128]{1,0:T(8,128)S(1)}, f32[8,128]{1,0:T(8,128)S(1)}, f32[256]{0:T(256)S(1)}, f32[256]{0:T(256...) custom-call(bf16[16,128]{1,0:T(8,128)(2,1)} %bitcast.8, ...), custom_call_target="tpu_custom_call" | custom-call | tf_op jit(solution)/shard_map/pallas_call | solution.py:26
  5.1 0.0 copy-start.2
  5.1 14.6 %all_to_all.35.x_ref = bf16[16,16,128]{2,1,0:T(8,128)(2,1)S(1)} all-to-all(bf16[16,16,128]{2,1,0:T(8,128)(2,1)S(1)} %get-tuple-element.22), channel_id=1, replica_groups=mesh['kv'=16,'z'=8,'core'=2] {'z','core'}, dimensions={0} | all-to-all | bytes 131072 | tf_op jit(solution)/shard_map/all_to_all | solution.py:258
  19.7 0.0 collective-permute-done.other_ref
  19.7 0.3 shard_map.141
  20.0 14.3 %all_to_all.36.parts_ref = bf16[16,8,896]{2,1,0:T(8,128)(2,1)S(1)} all-to-all(bf16[16,8,896]{2,1,0:T(8,128)(2,1)S(1)} %get-tuple-element.29), channel_id=1, replica_groups={{0,128,240,224,80,32,48,176,96,208,160,64,144,112,16,192},{1,129,241,22..., dimensions={0} | all-to-all | bytes 458752 | tf_op jit(solution)/shard_map/all_to_all | solution.py:258
  34.2 0.0 copy-done.2
  34.2 0.6 shard_map.142
  34.8 0.0 copy-start.4
  34.8 12.3 %all_to_all.37.merged_ref = bf16[32,8,256]{2,1,0:T(8,128)(2,1)S(1)} all-to-all(bf16[32,8,256]{2,1,0:T(8,128)(2,1)S(1)} %get-tuple-element.32), channel_id=1, replica_groups=mesh['kv'=16,'z'=8,'core'=2] {'kv','core'}, dimensions={0} | all-to-all | bytes 262144 | tf_op jit(solution)/shard_map/all_to_all | solution.py:258
  47.1 0.0 copy-done.4
  47.1 0.0 copy-start.1
  47.1 0.2 shard_map.143
  47.3 0.0 copy-start
  47.3 10.7 %all_to_all.38.parts_ref = bf16[8,128,128]{2,1,0:T(8,128)(2,1)S(1)} all-to-all(bf16[8,128,128]{2,1,0:T(8,128)(2,1)S(1)} %shard_map.143), channel_id=1, replica_groups={{0,2,8,6,4,10,14,12},{1,3,9,7,5,11,15,13},{16,18,24,22,20,26,30,28},{17..., dimensions={0} | all-to-all | bytes 524288 | tf_op jit(solution)/shard_map/all_to_all | solution.py:258
  58.0 0.0 copy-done.1
  58.0 0.0 copy-done
  58.0 3.1 %collective-permute-start.1 = (bf16[128,128]{1,0:T(8,128)(2,1)S(1)}, bf16[128,128]{1,0:T(8,128)(2,1)S(1)}, u32[]{:S(2)}, u32[]{:S(2)}) collective-permute-start(bf16[128,128]{1,0:T(8,128)(2,1)S(1)} %shard_map.144.half_ref), channel_id=1, source_target_pairs={{0,1},{1,0},{2,3},{3,2},{4,5},{5,4},{6,7},{7,6},{8,9},{9,8},{10,11... | collective-permute-start | bytes 98312 | tf_op jit(solution)/shard_map/ppermute | solution.py:343
  61.2 1.0 shard_map.145
  62.1 0.0 collective-permute-done.1.other_ref
  62.2 0.4 shard_map.146
  62.5 11.7 %all_to_all.39.parts_ref = bf16[16,8,1536]{2,1,0:T(8,128)(2,1)S(1)} all-to-all(bf16[16,8,1536]{2,1,0:T(8,128)(2,1)S(1)} %get-tuple-element.39), channel_id=1, replica_groups={{0,128,240,224,80,32,48,176,96,208,160,64,144,112,16,192},{1,129,241,22..., dimensions={0} | all-to-all | bytes 786432 | tf_op jit(solution)/shard_map/all_to_all | solution.py:258
  74.2 0.0 copy-start.3
  74.2 0.1 shard_map.147
  74.3 10.2 %all_to_all.40.hidden_ref = bf16[16,8,704]{2,1,0:T(8,128)(2,1)S(1)} all-to-all(bf16[16,8,704]{2,1,0:T(8,128)(2,1)S(1)} %shard_map.147), channel_id=1, replica_groups={{0,128,240,224,80,32,48,176,96,208,160,64,144,112,16,192},{1,129,241,22..., dimensions={0} | all-to-all | bytes 360448 | tf_op jit(solution)/shard_map/all_to_all | solution.py:258
  84.5 0.0 copy-done.3
  84.5 0.3 shard_map.148
  84.8 14.0 %all_to_all.41.parts_ref = bf16[16,16,128]{2,1,0:T(8,128)(2,1)S(1)} all-to-all(bf16[16,16,128]{2,1,0:T(8,128)(2,1)S(1)} %shard_map.148), channel_id=1, replica_groups=mesh['kv'=16,'z'=8,'core'=2] {'z','core'}, dimensions={0} | all-to-all | bytes 131072 | tf_op jit(solution)/shard_map/all_to_all | solution.py:258
  98.8 0.6 shard_map.149
  (1 shorter events, 0.0 us)
Async XLA Ops:
  0.6 19.0 %collective-permute-start = (bf16[256,256]{1,0:T(8,128)(2,1)}, bf16[256,256]{1,0:T(8,128)(2,1)S(1)}, u32[]{:S(2)}, u32[]{:S(2)}) collective-permute-start(bf16[256,256]{1,0:T(8,128)(2,1)} %own_ref.1), channel_id=1, source_target_pairs={{0,1},{1,0},{2,3},{3,2},{4,5},{5,4},{6,7},{7,6},{8,9},{9,8},{10,11... | collective-permute-start | bytes 393224 | tf_op jit(solution)/shard_map/ppermute | solution.py:309
  5.1 29.2 %copy-start.2 = (f32[8,1,128,256]{3,2,1,0:T(8,128)S(1)}, f32[8,1,128,256]{3,2,1,0:T(8,128)}, u32[]{:S(2)}) copy-start(f32[8,1,128,256]{3,2,1,0:T(8,128)} %state_ref.1) | copy-start | bytes 3145732
  34.8 12.3 %copy-start.4 = (bf16[256,256]{1,0:T(8,128)(2,1)S(1)}, bf16[256,256]{1,0:T(8,128)(2,1)}, u32[]{:S(2)}) copy-start(bf16[256,256]{1,0:T(8,128)(2,1)} %own_ref.1) | copy-start | bytes 393220
  47.1 10.9 %copy-start.1 = (bf16[256,704]{0,1:T(8,128)(2,1)S(1)}, bf16[256,704]{0,1:T(8,128)(2,1)}, u32[]{:S(2)}) copy-start(bf16[256,704]{0,1:T(8,128)(2,1)} %param.24) | copy-start | bytes 1081348
  47.3 10.7 %copy-start = (bf16[256,704]{0,1:T(8,128)(2,1)S(1)}, bf16[256,704]{0,1:T(8,128)(2,1)}, u32[]{:S(2)}) copy-start(bf16[256,704]{0,1:T(8,128)(2,1)} %param.23) | copy-start | bytes 1081348
  58.0 4.1 %collective-permute-start.1 = (bf16[128,128]{1,0:T(8,128)(2,1)S(1)}, bf16[128,128]{1,0:T(8,128)(2,1)S(1)}, u32[]{:S(2)}, u32[]{:S(2)}) collective-permute-start(bf16[128,128]{1,0:T(8,128)(2,1)S(1)} %shard_map.144.half_ref), channel_id=1, source_target_pairs={{0,1},{1,0},{2,3},{3,2},{4,5},{5,4},{6,7},{7,6},{8,9},{9,8},{10,11... | collective-permute-start | bytes 98312 | tf_op jit(solution)/shard_map/ppermute | solution.py:343
  74.2 10.3 %copy-start.3 = (bf16[704,256]{1,0:T(8,128)(2,1)S(1)}, bf16[704,256]{1,0:T(8,128)(2,1)}, u32[]{:S(2)}) copy-start(bf16[704,256]{1,0:T(8,128)(2,1)} %w_ref.1) | copy-start | bytes 1081348

commit v5 on v4

--- a/solution.py
+++ b/solution.py
@@ -16,10 +16,11 @@
 F32 = jnp.float32
 BF16 = jnp.bfloat16
 VMEM_BYTES = 8 << 20
+LONG = pl.CostEstimate(flops=4_000_000_000, bytes_accessed=8_000_000, transcendentals=0)
 FULL_VMEM_BYTES = 67_043_328 - 1_000_000
 
 
-def local_call(kernel, outs, *operands, scratch=(), space=pltpu.VMEM, out_space=pltpu.VMEM, limit=VMEM_BYTES):
+def local_call(kernel, outs, *operands, scratch=(), space=pltpu.VMEM, out_space=pltpu.VMEM, limit=VMEM_BYTES, cost=None):
     spaces = [space] * len(operands)
     several = isinstance(outs, tuple)
     vmem = pl.BlockSpec(memory_space=out_space)
@@ -29,6 +30,7 @@
         in_specs=[pl.BlockSpec(memory_space=s) for s in spaces],
         out_specs=tuple(vmem for _ in outs) if several else vmem,
         scratch_shapes=scratch,
+        cost_estimate=cost,
         compiler_params=pltpu.CompilerParams(vmem_limit_bytes=limit),
     )(*operands)
 
@@ -68,22 +70,22 @@
 
 
 def prepare(token_ref, length_ref, *refs):
-    count = (len(refs) - 6) // 2
-    sources, (copies_ref, sine_ref, cosine_ref), fetched = (
+    count = (len(refs) - 5) // 2
+    sources, (tokens_vmem, sine_ref, cosine_ref), fetched = (
         refs[:count],
         refs[count : count + 3],
         refs[count + 3 : 2 * count + 3],
     )
-    tokens_vmem, lengths_smem, sems = refs[2 * count + 3 :]
+    lengths_smem, sems = refs[2 * count + 3 :]
     copies = [
         pltpu.make_async_copy(source, target, sems.at[i])
         for i, (source, target) in enumerate(
-            zip((token_ref, length_ref, *sources), (tokens_vmem, lengths_smem, *fetched))
+            zip((length_ref, token_ref, *sources), (lengths_smem, tokens_vmem, *fetched))
         )
     ]
     for copy in copies:
         copy.start()
-    copies[1].wait()
+    copies[0].wait()
     shape = sine_ref.shape
     row = lax.broadcasted_iota(jnp.int32, shape, 0)
     position = jnp.zeros(shape, F32)
@@ -93,12 +95,14 @@
     first = lax.broadcasted_iota(jnp.int32, shape, 1) < QK // 2
     sine_ref[...] = jnp.where(first, -sine, sine)
     cosine_ref[...] = cosine
-    copies[0].wait()
-    tokens = tokens_vmem[...]
-    for i in range(copies_ref.shape[0]):
-        copies_ref[i] = tokens
-    for copy in copies[2:]:
+    for copy in copies[1:]:
         copy.wait()
+
+
+def spread(token_ref, out_ref):
+    tokens = token_ref[...]
+    for i in range(out_ref.shape[0]):
+        out_ref[i] = tokens
 
 
 def project(x_ref, gain_ref, q_ref, k_ref, v_ref, g_ref, out_ref, half_ref):
@@ -286,25 +290,28 @@
     along_kv = [list(kv_order(owners))]
 
     weights = (query_weight, key_weight, value_weight, gate_weight)
-    fetch = (mixer_gain, channel_gain, *weights)
-    copies, sine, cosine, mixer_gain, channel_gain, *weights = local_call(
+    own, sine, cosine, mixer_gain, channel_gain = local_call(
         prepare,
         (
-            shaped((members, own_width, batch), BF16),
+            shaped((own_width, batch), BF16),
             shaped((rows, QK), F32),
             shaped((rows, QK), F32),
-            *(shaped(a.shape, a.dtype) for a in fetch),
+            shaped(mixer_gain.shape, F32),
+            shaped(channel_gain.shape, F32),
         ),
         tokens.T,
         lengths,
-        *fetch,
+        mixer_gain,
+        channel_gain,
         scratch=(
-            pltpu.VMEM((own_width, batch), BF16),
             pltpu.SMEM((rows,), jnp.int32),
-            pltpu.SemaphoreType.DMA((len(fetch) + 2,)),
+            pltpu.SemaphoreType.DMA((4,)),
         ),
         space=pltpu.HBM,
         limit=FULL_VMEM_BYTES,
+    )
+    copies = local_call(
+        spread, shaped((members, own_width, batch), BF16), own, cost=LONG
     )
     other_weight = lax.ppermute(output_weight, "core", swap)
     features = exchanged(copies, ("z", "core"))

time: 99.8 us -> 99.5 us (level)
    pallas_call x10 -> x11, Pallas kernels: 4.58 us -> 4.19 us  [local_call(): pl.pallas_call(kernel, out_shape=outs, in_specs=[pl.BlockSpec(memory_spac...]
where the time goes in v5:
time: 99.5 us; the launch traced here: 99.1 us
  blocking collectives  87.6 us (88%)
  starting transfers between devices  6.42 us (6%)
  Pallas kernels  4.19 us (4%)
    all_to_all x7, blocking collectives, exchanged(): lax.all_to_all(blocks, axis, 0, 0, tiled=True, axis_index_groups=groups)  87.6 us
    pallas_call x11, Pallas kernels, local_call(): pl.pallas_call(kernel, out_shape=outs, in_specs=[pl.BlockSpec(memory_spac...  4.19 us
    ppermute x1, starting transfers between devices, on_device(): other_weight = lax.ppermute(output_weight, 'core', swap)  3.29 us
    ppermute x1, starting transfers between devices, on_device(): residual_other = lax.ppermute(residual_half, 'core', swap)  3.14 us
  transfers between devices with their start and end apart: 2, of which 0 were waited for; matrix products, arithmetic and copies ran while one was open for 0% of the time, Pallas kernels for 2%

profile of v5, /device:TPU:1, one launch (start us, length us, event | category | flops | bytes accessed | tf_op | source)
XLA Modules:
  0.0 99.1 jit_solution(9276904967175736598)
XLA Ops:
  0.6 3.3 %collective-permute-start = (bf16[256,256]{1,0:T(8,128)(2,1)}, bf16[256,256]{1,0:T(8,128)(2,1)S(1)}, u32[]{:S(2)}, u32[]{:S(2)}) collective-permute-start(bf16[256,256]{1,0:T(8,128)(2,1)} %own_ref.1), channel_id=1, source_target_pairs={{0,1},{1,0},{2,3},{3,2},{4,5},{5,4},{6,7},{7,6},{8,9},{9,8},{10,11... | collective-permute-start | bytes 393224 | tf_op jit(solution)/shard_map/ppermute | solution.py:316
  3.9 0.7 shard_map.140
  4.7 0.0 copy-start.4
  4.7 0.0 copy-start.5
  4.7 0.0 copy-start.7
  4.7 0.0 copy-start.8
  4.7 0.0 copy-start.2
  4.8 14.6 %all_to_all.35.x_ref = bf16[16,16,128]{2,1,0:T(8,128)(2,1)S(1)} all-to-all(bf16[16,16,128]{2,1,0:T(8,128)(2,1)S(1)} %shard_map.141), channel_id=1, replica_groups=mesh['kv'=16,'z'=8,'core'=2] {'z','core'}, dimensions={0} | all-to-all | bytes 131072 | tf_op jit(solution)/shard_map/all_to_all | solution.py:262
  19.3 0.0 collective-permute-done.other_ref
  19.3 0.0 copy-done.4
  19.3 0.0 copy-done.5
  19.3 0.0 copy-done.7
  19.4 0.0 copy-done.8
  19.4 0.3 shard_map.142
  19.6 14.3 %all_to_all.36.parts_ref = bf16[16,8,896]{2,1,0:T(8,128)(2,1)S(1)} all-to-all(bf16[16,8,896]{2,1,0:T(8,128)(2,1)S(1)} %get-tuple-element.21), channel_id=1, replica_groups={{0,128,240,224,80,32,48,176,96,208,160,64,144,112,16,192},{1,129,241,22..., dimensions={0} | all-to-all | bytes 458752 | tf_op jit(solution)/shard_map/all_to_all | solution.py:262
  33.9 0.0 copy-done.2
  33.9 0.6 shard_map.143
  34.5 0.0 copy-start.6
  34.5 12.3 %all_to_all.37.merged_ref = bf16[32,8,256]{2,1,0:T(8,128)(2,1)S(1)} all-to-all(bf16[32,8,256]{2,1,0:T(8,128)(2,1)S(1)} %get-tuple-element.24), channel_id=1, replica_groups=mesh['kv'=16,'z'=8,'core'=2] {'kv','core'}, dimensions={0} | all-to-all | bytes 262144 | tf_op jit(solution)/shard_map/all_to_all | solution.py:262
  46.8 0.0 copy-done.6
  46.8 0.0 copy-start.1
  46.8 0.2 shard_map.144
  47.0 0.0 copy-start
  47.0 10.7 %all_to_all.38.parts_ref = bf16[8,128,128]{2,1,0:T(8,128)(2,1)S(1)} all-to-all(bf16[8,128,128]{2,1,0:T(8,128)(2,1)S(1)} %shard_map.144), channel_id=1, replica_groups={{0,2,8,6,4,10,14,12},{1,3,9,7,5,11,15,13},{16,18,24,22,20,26,30,28},{17..., dimensions={0} | all-to-all | bytes 524288 | tf_op jit(solution)/shard_map/all_to_all | solution.py:262
  57.7 0.0 copy-done.1
  57.7 0.0 copy-done
  57.7 3.1 %collective-permute-start.1 = (bf16[128,128]{1,0:T(8,128)(2,1)S(1)}, bf16[128,128]{1,0:T(8,128)(2,1)S(1)}, u32[]{:S(2)}, u32[]{:S(2)}) collective-permute-start(bf16[128,128]{1,0:T(8,128)(2,1)S(1)} %shard_map.145.half_ref), channel_id=1, source_target_pairs={{0,1},{1,0},{2,3},{3,2},{4,5},{5,4},{6,7},{7,6},{8,9},{9,8},{10,11... | collective-permute-start | bytes 98312 | tf_op jit(solution)/shard_map/ppermute | solution.py:350
  60.8 1.0 shard_map.146
  61.8 0.0 collective-permute-done.1.other_ref
  61.8 0.4 shard_map.147
  62.2 11.7 %all_to_all.39.parts_ref = bf16[16,8,1536]{2,1,0:T(8,128)(2,1)S(1)} all-to-all(bf16[16,8,1536]{2,1,0:T(8,128)(2,1)S(1)} %get-tuple-element.31), channel_id=1, replica_groups={{0,128,240,224,80,32,48,176,96,208,160,64,144,112,16,192},{1,129,241,22..., dimensions={0} | all-to-all | bytes 786432 | tf_op jit(solution)/shard_map/all_to_all | solution.py:262
  73.9 0.0 copy-start.3
  73.9 0.1 shard_map.148
  74.0 10.2 %all_to_all.40.hidden_ref = bf16[16,8,704]{2,1,0:T(8,128)(2,1)S(1)} all-to-all(bf16[16,8,704]{2,1,0:T(8,128)(2,1)S(1)} %shard_map.148), channel_id=1, replica_groups={{0,128,240,224,80,32,48,176,96,208,160,64,144,112,16,192},{1,129,241,22..., dimensions={0} | all-to-all | bytes 360448 | tf_op jit(solution)/shard_map/all_to_all | solution.py:262
  84.2 0.0 copy-done.3
  84.2 0.3 shard_map.149
  84.5 14.0 %all_to_all.41.parts_ref = bf16[16,16,128]{2,1,0:T(8,128)(2,1)S(1)} all-to-all(bf16[16,16,128]{2,1,0:T(8,128)(2,1)S(1)} %shard_map.149), channel_id=1, replica_groups=mesh['kv'=16,'z'=8,'core'=2] {'z','core'}, dimensions={0} | all-to-all | bytes 131072 | tf_op jit(solution)/shard_map/all_to_all | solution.py:262
  98.5 0.6 shard_map.150
  (2 shorter events, 0.1 us)
Async XLA Ops:
  0.6 18.7 %collective-permute-start = (bf16[256,256]{1,0:T(8,128)(2,1)}, bf16[256,256]{1,0:T(8,128)(2,1)S(1)}, u32[]{:S(2)}, u32[]{:S(2)}) collective-permute-start(bf16[256,256]{1,0:T(8,128)(2,1)} %own_ref.1), channel_id=1, source_target_pairs={{0,1},{1,0},{2,3},{3,2},{4,5},{5,4},{6,7},{7,6},{8,9},{9,8},{10,11... | collective-permute-start | bytes 393224 | tf_op jit(solution)/shard_map/ppermute | solution.py:316
  4.7 14.7 %copy-start.4 = (bf16[256,256]{1,0:T(8,128)(2,1)S(1)}, bf16[256,256]{1,0:T(8,128)(2,1)}, u32[]{:S(2)}) copy-start(bf16[256,256]{1,0:T(8,128)(2,1)} %v_ref.1) | copy-start | bytes 393220
  4.7 14.7 %copy-start.5 = (bf16[256,256]{1,0:T(8,128)(2,1)S(1)}, bf16[256,256]{1,0:T(8,128)(2,1)}, u32[]{:S(2)}) copy-start(bf16[256,256]{1,0:T(8,128)(2,1)} %g_ref.1) | copy-start | bytes 393220
  4.7 14.7 %copy-start.7 = (bf16[256,128]{1,0:T(8,128)(2,1)S(1)}, bf16[256,128]{1,0:T(8,128)(2,1)}, u32[]{:S(2)}) copy-start(bf16[256,128]{1,0:T(8,128)(2,1)} %q_ref.1) | copy-start | bytes 196612
  4.7 14.6 %copy-start.8 = (bf16[256,128]{1,0:T(8,128)(2,1)S(1)}, bf16[256,128]{1,0:T(8,128)(2,1)}, u32[]{:S(2)}) copy-start(bf16[256,128]{1,0:T(8,128)(2,1)} %k_ref.1) | copy-start | bytes 196612
  4.7 29.2 %copy-start.2 = (f32[8,1,128,256]{3,2,1,0:T(8,128)S(1)}, f32[8,1,128,256]{3,2,1,0:T(8,128)}, u32[]{:S(2)}) copy-start(f32[8,1,128,256]{3,2,1,0:T(8,128)} %state_ref.1) | copy-start | bytes 3145732
  34.5 12.3 %copy-start.6 = (bf16[256,256]{1,0:T(8,128)(2,1)S(1)}, bf16[256,256]{1,0:T(8,128)(2,1)}, u32[]{:S(2)}) copy-start(bf16[256,256]{1,0:T(8,128)(2,1)} %own_ref.1) | copy-start | bytes 393220
  46.8 10.9 %copy-start.1 = (bf16[256,704]{0,1:T(8,128)(2,1)S(1)}, bf16[256,704]{0,1:T(8,128)(2,1)}, u32[]{:S(2)}) copy-start(bf16[256,704]{0,1:T(8,128)(2,1)} %param.24) | copy-start | bytes 1081348
  47.0 10.7 %copy-start = (bf16[256,704]{0,1:T(8,128)(2,1)S(1)}, bf16[256,704]{0,1:T(8,128)(2,1)}, u32[]{:S(2)}) copy-start(bf16[256,704]{0,1:T(8,128)(2,1)} %param.23) | copy-start | bytes 1081348
  57.7 4.1 %collective-permute-start.1 = (bf16[128,128]{1,0:T(8,128)(2,1)S(1)}, bf16[128,128]{1,0:T(8,128)(2,1)S(1)}, u32[]{:S(2)}, u32[]{:S(2)}) collective-permute-start(bf16[128,128]{1,0:T(8,128)(2,1)S(1)} %shard_map.145.half_ref), channel_id=1, source_target_pairs={{0,1},{1,0},{2,3},{3,2},{4,5},{5,4},{6,7},{7,6},{8,9},{9,8},{10,11... | collective-permute-start | bytes 98312 | tf_op jit(solution)/shard_map/ppermute | solution.py:350
  73.9 10.3 %copy-start.3 = (bf16[704,256]{1,0:T(8,128)(2,1)S(1)}, bf16[704,256]{1,0:T(8,128)(2,1)}, u32[]{:S(2)}) copy-start(bf16[704,256]{1,0:T(8,128)(2,1)} %w_ref.1) | copy-start | bytes 1081348

commit v6 on v5

--- a/solution.py
+++ b/solution.py
@@ -12,6 +12,7 @@
 QK = 128
 VD = 256
 LANES = 128
+TP_ORDER = (1, 0, 2, 3, 4, 5, 6, 7, 8, 9, 10, 11, 12, 13, 14, 15)
 KV_ORDER = (0, 8, 15, 14, 5, 2, 3, 11, 6, 13, 10, 4, 9, 7, 1, 12)
 F32 = jnp.float32
 BF16 = jnp.bfloat16
@@ -45,6 +46,10 @@
 
 def kv_order(owners):
     return KV_ORDER if owners == len(KV_ORDER) else tuple(range(owners))
+
+
+def tp_order(members):
+    return TP_ORDER if members == len(TP_ORDER) else tuple(range(members))
 
 
 def store_rows(out_ref, value, start):
@@ -251,7 +256,10 @@
 
 def contract_units(hidden_ref, w_ref, out_ref):
     down = jnp.dot(all_rows(hidden_ref).astype(BF16), w_ref[...], preferred_element_type=F32)
-    out_ref[...] = down.T.astype(BF16).reshape(out_ref.shape)
+    down = down.T.astype(BF16)
+    each = out_ref.shape[1]
+    for at, owner in enumerate(tp_order(out_ref.shape[0])):
+        out_ref[at] = down[owner * each : (owner + 1) * each]
 
 
 def finish(parts_ref, mine_ref, out_ref):
@@ -376,7 +384,7 @@
         ffn_down,
     )
     layer_output = local_call(
-        finish, jax.ShapeDtypeStruct((own_width, batch), BF16), exchanged(down, ("z", "core")), mine
+        finish, jax.ShapeDtypeStruct((own_width, batch), BF16), exchanged(down, ("z", "core"), [list(tp_order(members))]), mine
     )
     return (layer_output.T, new_state)
 

time: 99.5 us -> 98.8 us (level)
  no operation moved by 1% of the time
where the time goes in v6:
time: 98.8 us; the launch traced here: 98.4 us
  blocking collectives  86.9 us (88%)
  starting transfers between devices  6.42 us (6%)
  Pallas kernels  4.19 us (4%)
    all_to_all x7, blocking collectives, exchanged(): lax.all_to_all(blocks, axis, 0, 0, tiled=True, axis_index_groups=groups)  86.9 us
    pallas_call x11, Pallas kernels, local_call(): pl.pallas_call(kernel, out_shape=outs, in_specs=[pl.BlockSpec(memory_spac...  4.19 us
    ppermute x1, starting transfers between devices, on_device(): other_weight = lax.ppermute(output_weight, 'core', swap)  3.29 us
    ppermute x1, starting transfers between devices, on_device(): residual_other = lax.ppermute(residual_half, 'core', swap)  3.14 us
  transfers between devices with their start and end apart: 2, of which 0 were waited for; matrix products, arithmetic and copies ran while one was open for 0% of the time, Pallas kernels for 2%

profile of v6, /device:TPU:1, one launch (start us, length us, event | category | flops | bytes accessed | tf_op | source)
XLA Modules:
  0.0 98.4 jit_solution(13298829622484067524)
XLA Ops:
  0.6 3.3 %collective-permute-start = (bf16[256,256]{1,0:T(8,128)(2,1)}, bf16[256,256]{1,0:T(8,128)(2,1)S(1)}, u32[]{:S(2)}, u32[]{:S(2)}) collective-permute-start(bf16[256,256]{1,0:T(8,128)(2,1)} %own_ref.1), channel_id=1, source_target_pairs={{0,1},{1,0},{2,3},{3,2},{4,5},{5,4},{6,7},{7,6},{8,9},{9,8},{10,11... | collective-permute-start | bytes 393224 | tf_op jit(solution)/shard_map/ppermute | solution.py:324
  3.9 0.7 shard_map.140
  4.7 0.0 copy-start.4
  4.7 0.0 copy-start.5
  4.7 0.0 copy-start.7
  4.7 0.0 copy-start.8
  4.7 0.0 copy-start.2
  4.8 14.6 %all_to_all.35.x_ref = bf16[16,16,128]{2,1,0:T(8,128)(2,1)S(1)} all-to-all(bf16[16,16,128]{2,1,0:T(8,128)(2,1)S(1)} %shard_map.141), channel_id=1, replica_groups=mesh['kv'=16,'z'=8,'core'=2] {'z','core'}, dimensions={0} | all-to-all | bytes 131072 | tf_op jit(solution)/shard_map/all_to_all | solution.py:270
  19.3 0.0 collective-permute-done.other_ref
  19.3 0.0 copy-done.4
  19.3 0.0 copy-done.5
  19.3 0.0 copy-done.7
  19.4 0.0 copy-done.8
  19.4 0.3 shard_map.142
  19.6 14.3 %all_to_all.36.parts_ref = bf16[16,8,896]{2,1,0:T(8,128)(2,1)S(1)} all-to-all(bf16[16,8,896]{2,1,0:T(8,128)(2,1)S(1)} %get-tuple-element.21), channel_id=1, replica_groups={{0,128,240,224,80,32,48,176,96,208,160,64,144,112,16,192},{1,129,241,22..., dimensions={0} | all-to-all | bytes 458752 | tf_op jit(solution)/shard_map/all_to_all | solution.py:270
  33.9 0.0 copy-done.2
  33.9 0.6 shard_map.143
  34.5 0.0 copy-start.6
  34.5 12.3 %all_to_all.37.merged_ref = bf16[32,8,256]{2,1,0:T(8,128)(2,1)S(1)} all-to-all(bf16[32,8,256]{2,1,0:T(8,128)(2,1)S(1)} %get-tuple-element.24), channel_id=1, replica_groups=mesh['kv'=16,'z'=8,'core'=2] {'kv','core'}, dimensions={0} | all-to-all | bytes 262144 | tf_op jit(solution)/shard_map/all_to_all | solution.py:270
  46.8 0.0 copy-done.6
  46.8 0.0 copy-start.1
  46.8 0.2 shard_map.144
  47.0 0.0 copy-start
  47.0 10.7 %all_to_all.38.parts_ref = bf16[8,128,128]{2,1,0:T(8,128)(2,1)S(1)} all-to-all(bf16[8,128,128]{2,1,0:T(8,128)(2,1)S(1)} %shard_map.144), channel_id=1, replica_groups={{0,2,8,6,4,10,14,12},{1,3,9,7,5,11,15,13},{16,18,24,22,20,26,30,28},{17..., dimensions={0} | all-to-all | bytes 524288 | tf_op jit(solution)/shard_map/all_to_all | solution.py:270
  57.7 0.0 copy-done.1
  57.7 0.0 copy-done
  57.7 3.1 %collective-permute-start.1 = (bf16[128,128]{1,0:T(8,128)(2,1)S(1)}, bf16[128,128]{1,0:T(8,128)(2,1)S(1)}, u32[]{:S(2)}, u32[]{:S(2)}) collective-permute-start(bf16[128,128]{1,0:T(8,128)(2,1)S(1)} %shard_map.145.half_ref), channel_id=1, source_target_pairs={{0,1},{1,0},{2,3},{3,2},{4,5},{5,4},{6,7},{7,6},{8,9},{9,8},{10,11... | collective-permute-start | bytes 98312 | tf_op jit(solution)/shard_map/ppermute | solution.py:358
  60.8 1.0 shard_map.146
  61.8 0.0 collective-permute-done.1.other_ref
  61.8 0.4 shard_map.147
  62.2 11.7 %all_to_all.39.parts_ref = bf16[16,8,1536]{2,1,0:T(8,128)(2,1)S(1)} all-to-all(bf16[16,8,1536]{2,1,0:T(8,128)(2,1)S(1)} %get-tuple-element.31), channel_id=1, replica_groups={{0,128,240,224,80,32,48,176,96,208,160,64,144,112,16,192},{1,129,241,22..., dimensions={0} | all-to-all | bytes 786432 | tf_op jit(solution)/shard_map/all_to_all | solution.py:270
  73.9 0.0 copy-start.3
  73.9 0.1 shard_map.148
  74.0 10.2 %all_to_all.40.hidden_ref = bf16[16,8,704]{2,1,0:T(8,128)(2,1)S(1)} all-to-all(bf16[16,8,704]{2,1,0:T(8,128)(2,1)S(1)} %shard_map.148), channel_id=1, replica_groups={{0,128,240,224,80,32,48,176,96,208,160,64,144,112,16,192},{1,129,241,22..., dimensions={0} | all-to-all | bytes 360448 | tf_op jit(solution)/shard_map/all_to_all | solution.py:270
  84.2 0.0 copy-done.3
  84.2 0.3 shard_map.149
  84.5 13.2 %all_to_all.41.parts_ref = bf16[16,16,128]{2,1,0:T(8,128)(2,1)S(1)} all-to-all(bf16[16,16,128]{2,1,0:T(8,128)(2,1)S(1)} %shard_map.149), channel_id=1, replica_groups={{1,0,2,3,4,5,6,7,8,9,10,11,12,13,14,15},{17,16,18,19,20,21,22,23,24,25,..., dimensions={0} | all-to-all | bytes 131072 | tf_op jit(solution)/shard_map/all_to_all | solution.py:270
  97.7 0.6 shard_map.150
  (2 shorter events, 0.1 us)
Async XLA Ops:
  0.6 18.7 %collective-permute-start = (bf16[256,256]{1,0:T(8,128)(2,1)}, bf16[256,256]{1,0:T(8,128)(2,1)S(1)}, u32[]{:S(2)}, u32[]{:S(2)}) collective-permute-start(bf16[256,256]{1,0:T(8,128)(2,1)} %own_ref.1), channel_id=1, source_target_pairs={{0,1},{1,0},{2,3},{3,2},{4,5},{5,4},{6,7},{7,6},{8,9},{9,8},{10,11... | collective-permute-start | bytes 393224 | tf_op jit(solution)/shard_map/ppermute | solution.py:324
  4.7 14.7 %copy-start.4 = (bf16[256,256]{1,0:T(8,128)(2,1)S(1)}, bf16[256,256]{1,0:T(8,128)(2,1)}, u32[]{:S(2)}) copy-start(bf16[256,256]{1,0:T(8,128)(2,1)} %v_ref.1) | copy-start | bytes 393220
  4.7 14.7 %copy-start.5 = (bf16[256,256]{1,0:T(8,128)(2,1)S(1)}, bf16[256,256]{1,0:T(8,128)(2,1)}, u32[]{:S(2)}) copy-start(bf16[256,256]{1,0:T(8,128)(2,1)} %g_ref.1) | copy-start | bytes 393220
  4.7 14.7 %copy-start.7 = (bf16[256,128]{1,0:T(8,128)(2,1)S(1)}, bf16[256,128]{1,0:T(8,128)(2,1)}, u32[]{:S(2)}) copy-start(bf16[256,128]{1,0:T(8,128)(2,1)} %q_ref.1) | copy-start | bytes 196612
  4.7 14.6 %copy-start.8 = (bf16[256,128]{1,0:T(8,128)(2,1)S(1)}, bf16[256,128]{1,0:T(8,128)(2,1)}, u32[]{:S(2)}) copy-start(bf16[256,128]{1,0:T(8,128)(2,1)} %k_ref.1) | copy-start | bytes 196612
  4.7 29.2 %copy-start.2 = (f32[8,1,128,256]{3,2,1,0:T(8,128)S(1)}, f32[8,1,128,256]{3,2,1,0:T(8,128)}, u32[]{:S(2)}) copy-start(f32[8,1,128,256]{3,2,1,0:T(8,128)} %state_ref.1) | copy-start | bytes 3145732
  34.5 12.3 %copy-start.6 = (bf16[256,256]{1,0:T(8,128)(2,1)S(1)}, bf16[256,256]{1,0:T(8,128)(2,1)}, u32[]{:S(2)}) copy-start(bf16[256,256]{1,0:T(8,128)(2,1)} %own_ref.1) | copy-start | bytes 393220
  46.8 10.9 %copy-start.1 = (bf16[256,704]{0,1:T(8,128)(2,1)S(1)}, bf16[256,704]{0,1:T(8,128)(2,1)}, u32[]{:S(2)}) copy-start(bf16[256,704]{0,1:T(8,128)(2,1)} %param.24) | copy-start | bytes 1081348
  47.0 10.7 %copy-start = (bf16[256,704]{0,1:T(8,128)(2,1)S(1)}, bf16[256,704]{0,1:T(8,128)(2,1)}, u32[]{:S(2)}) copy-start(bf16[256,704]{0,1:T(8,128)(2,1)} %param.23) | copy-start | bytes 1081348
  57.7 4.1 %collective-permute-start.1 = (bf16[128,128]{1,0:T(8,128)(2,1)S(1)}, bf16[128,128]{1,0:T(8,128)(2,1)S(1)}, u32[]{:S(2)}, u32[]{:S(2)}) collective-permute-start(bf16[128,128]{1,0:T(8,128)(2,1)S(1)} %shard_map.145.half_ref), channel_id=1, source_target_pairs={{0,1},{1,0},{2,3},{3,2},{4,5},{5,4},{6,7},{7,6},{8,9},{9,8},{10,11... | collective-permute-start | bytes 98312 | tf_op jit(solution)/shard_map/ppermute | solution.py:358
  73.9 10.3 %copy-start.3 = (bf16[704,256]{1,0:T(8,128)(2,1)S(1)}, bf16[704,256]{1,0:T(8,128)(2,1)}, u32[]{:S(2)}) copy-start(bf16[704,256]{1,0:T(8,128)(2,1)} %w_ref.1) | copy-start | bytes 1081348

commit v7 on v6

--- a/solution.py
+++ b/solution.py
@@ -294,7 +294,7 @@
     middle = -(-(units + 1) // LANES) * LANES
     swap = [(0, 1), (1, 0)]
     gate_rows, up_rows = ffn_gate.T, ffn_up.T
-    along_z = [[0, 1, 4, 3, 2, 5, 7, 6]] if chips == 8 else None
+    along_z = [[3 * i % chips for i in range(chips)]]
     along_kv = [list(kv_order(owners))]
 
     weights = (query_weight, key_weight, value_weight, gate_weight)

time: 98.8 us -> 98.8 us (level)
  starting transfers between devices: 6.42 us -> 5.08 us
  blocking collectives: 86.9 us -> 88.2 us
    all_to_all x7, blocking collectives: 86.9 us -> 88.2 us  [exchanged(): lax.all_to_all(blocks, axis, 0, 0, tiled=True, axis_index_groups=groups)]
    ppermute x1, starting transfers between devices: 3.14 us -> 1.79 us  [on_device(): residual_other = lax.ppermute(residual_half, 'core', swap)]
where the time goes in v7:
time: 98.8 us; the launch traced here: 98.4 us
  blocking collectives  88.2 us (89%)
  starting transfers between devices  5.08 us (5%)
  Pallas kernels  4.19 us (4%)
    all_to_all x7, blocking collectives, exchanged(): lax.all_to_all(blocks, axis, 0, 0, tiled=True, axis_index_groups=groups)  88.2 us
    pallas_call x11, Pallas kernels, local_call(): pl.pallas_call(kernel, out_shape=outs, in_specs=[pl.BlockSpec(memory_spac...  4.19 us
    ppermute x1, starting transfers between devices, on_device(): other_weight = lax.ppermute(output_weight, 'core', swap)  3.29 us
  transfers between devices with their start and end apart: 2, of which 0 were waited for; matrix products, arithmetic and copies ran while one was open for 0% of the time, Pallas kernels for 2%

profile of v7, /device:TPU:1, one launch (start us, length us, event | category | flops | bytes accessed | tf_op | source)
XLA Modules:
  0.0 98.4 jit_solution(3627444365655716839)
XLA Ops:
  0.6 3.3 %collective-permute-start = (bf16[256,256]{1,0:T(8,128)(2,1)}, bf16[256,256]{1,0:T(8,128)(2,1)S(1)}, u32[]{:S(2)}, u32[]{:S(2)}) collective-permute-start(bf16[256,256]{1,0:T(8,128)(2,1)} %own_ref.1), channel_id=1, source_target_pairs={{0,1},{1,0},{2,3},{3,2},{4,5},{5,4},{6,7},{7,6},{8,9},{9,8},{10,11... | collective-permute-start | bytes 393224 | tf_op jit(solution)/shard_map/ppermute | solution.py:324
  3.9 0.7 shard_map.140
  4.7 0.0 copy-start.4
  4.7 0.0 copy-start.5
  4.7 0.0 copy-start.7
  4.7 0.0 copy-start.8
  4.7 0.0 copy-start.2
  4.8 14.6 %all_to_all.35.x_ref = bf16[16,16,128]{2,1,0:T(8,128)(2,1)S(1)} all-to-all(bf16[16,16,128]{2,1,0:T(8,128)(2,1)S(1)} %shard_map.141), channel_id=1, replica_groups=mesh['kv'=16,'z'=8,'core'=2] {'z','core'}, dimensions={0} | all-to-all | bytes 131072 | tf_op jit(solution)/shard_map/all_to_all | solution.py:270
  19.3 0.0 collective-permute-done.other_ref
  19.3 0.0 copy-done.4
  19.3 0.0 copy-done.5
  19.3 0.0 copy-done.7
  19.4 0.0 copy-done.8
  19.4 0.3 shard_map.142
  19.6 14.3 %all_to_all.36.parts_ref = bf16[16,8,896]{2,1,0:T(8,128)(2,1)S(1)} all-to-all(bf16[16,8,896]{2,1,0:T(8,128)(2,1)S(1)} %get-tuple-element.21), channel_id=1, replica_groups={{0,128,240,224,80,32,48,176,96,208,160,64,144,112,16,192},{1,129,241,22..., dimensions={0} | all-to-all | bytes 458752 | tf_op jit(solution)/shard_map/all_to_all | solution.py:270
  33.9 0.0 copy-done.2
  33.9 0.6 shard_map.143
  34.5 0.0 copy-start.6
  34.5 12.3 %all_to_all.37.merged_ref = bf16[32,8,256]{2,1,0:T(8,128)(2,1)S(1)} all-to-all(bf16[32,8,256]{2,1,0:T(8,128)(2,1)S(1)} %get-tuple-element.24), channel_id=1, replica_groups=mesh['kv'=16,'z'=8,'core'=2] {'kv','core'}, dimensions={0} | all-to-all | bytes 262144 | tf_op jit(solution)/shard_map/all_to_all | solution.py:270
  46.8 0.0 copy-done.6
  46.8 0.0 copy-start.1
  46.8 0.2 shard_map.144
  47.0 0.0 copy-start
  47.0 13.0 %all_to_all.38.parts_ref = bf16[8,128,128]{2,1,0:T(8,128)(2,1)S(1)} all-to-all(bf16[8,128,128]{2,1,0:T(8,128)(2,1)S(1)} %shard_map.144), channel_id=1, replica_groups={{0,6,12,2,8,14,4,10},{1,7,13,3,9,15,5,11},{16,22,28,18,24,30,20,26},{17..., dimensions={0} | all-to-all | bytes 524288 | tf_op jit(solution)/shard_map/all_to_all | solution.py:270
  60.0 0.0 copy-done.1
  60.0 0.0 copy-done
  60.0 1.8 %collective-permute-start.1 = (bf16[128,128]{1,0:T(8,128)(2,1)S(1)}, bf16[128,128]{1,0:T(8,128)(2,1)S(1)}, u32[]{:S(2)}, u32[]{:S(2)}) collective-permute-start(bf16[128,128]{1,0:T(8,128)(2,1)S(1)} %shard_map.145.half_ref), channel_id=1, source_target_pairs={{0,1},{1,0},{2,3},{3,2},{4,5},{5,4},{6,7},{7,6},{8,9},{9,8},{10,11... | collective-permute-start | bytes 98312 | tf_op jit(solution)/shard_map/ppermute | solution.py:358
  61.8 1.0 shard_map.146
  62.8 0.0 collective-permute-done.1.other_ref
  62.8 0.4 shard_map.147
  63.2 11.7 %all_to_all.39.parts_ref = bf16[16,8,1536]{2,1,0:T(8,128)(2,1)S(1)} all-to-all(bf16[16,8,1536]{2,1,0:T(8,128)(2,1)S(1)} %get-tuple-element.31), channel_id=1, replica_groups={{0,128,240,224,80,32,48,176,96,208,160,64,144,112,16,192},{1,129,241,22..., dimensions={0} | all-to-all | bytes 786432 | tf_op jit(solution)/shard_map/all_to_all | solution.py:270
  74.8 0.0 copy-start.3
  74.8 0.1 shard_map.148
  75.0 10.2 %all_to_all.40.hidden_ref = bf16[16,8,704]{2,1,0:T(8,128)(2,1)S(1)} all-to-all(bf16[16,8,704]{2,1,0:T(8,128)(2,1)S(1)} %shard_map.148), channel_id=1, replica_groups={{0,128,240,224,80,32,48,176,96,208,160,64,144,112,16,192},{1,129,241,22..., dimensions={0} | all-to-all | bytes 360448 | tf_op jit(solution)/shard_map/all_to_all | solution.py:270
  85.1 0.0 copy-done.3
  85.2 0.3 shard_map.149
  85.5 12.3 %all_to_all.41.parts_ref = bf16[16,16,128]{2,1,0:T(8,128)(2,1)S(1)} all-to-all(bf16[16,16,128]{2,1,0:T(8,128)(2,1)S(1)} %shard_map.149), channel_id=1, replica_groups={{1,0,2,3,4,5,6,7,8,9,10,11,12,13,14,15},{17,16,18,19,20,21,22,23,24,25,..., dimensions={0} | all-to-all | bytes 131072 | tf_op jit(solution)/shard_map/all_to_all | solution.py:270
  97.8 0.6 shard_map.150
  (2 shorter events, 0.1 us)
Async XLA Ops:
  0.6 18.7 %collective-permute-start = (bf16[256,256]{1,0:T(8,128)(2,1)}, bf16[256,256]{1,0:T(8,128)(2,1)S(1)}, u32[]{:S(2)}, u32[]{:S(2)}) collective-permute-start(bf16[256,256]{1,0:T(8,128)(2,1)} %own_ref.1), channel_id=1, source_target_pairs={{0,1},{1,0},{2,3},{3,2},{4,5},{5,4},{6,7},{7,6},{8,9},{9,8},{10,11... | collective-permute-start | bytes 393224 | tf_op jit(solution)/shard_map/ppermute | solution.py:324
  4.7 14.7 %copy-start.4 = (bf16[256,256]{1,0:T(8,128)(2,1)S(1)}, bf16[256,256]{1,0:T(8,128)(2,1)}, u32[]{:S(2)}) copy-start(bf16[256,256]{1,0:T(8,128)(2,1)} %v_ref.1) | copy-start | bytes 393220
  4.7 14.7 %copy-start.5 = (bf16[256,256]{1,0:T(8,128)(2,1)S(1)}, bf16[256,256]{1,0:T(8,128)(2,1)}, u32[]{:S(2)}) copy-start(bf16[256,256]{1,0:T(8,128)(2,1)} %g_ref.1) | copy-start | bytes 393220
  4.7 14.7 %copy-start.7 = (bf16[256,128]{1,0:T(8,128)(2,1)S(1)}, bf16[256,128]{1,0:T(8,128)(2,1)}, u32[]{:S(2)}) copy-start(bf16[256,128]{1,0:T(8,128)(2,1)} %q_ref.1) | copy-start | bytes 196612
  4.7 14.6 %copy-start.8 = (bf16[256,128]{1,0:T(8,128)(2,1)S(1)}, bf16[256,128]{1,0:T(8,128)(2,1)}, u32[]{:S(2)}) copy-start(bf16[256,128]{1,0:T(8,128)(2,1)} %k_ref.1) | copy-start | bytes 196612
  4.7 29.2 %copy-start.2 = (f32[8,1,128,256]{3,2,1,0:T(8,128)S(1)}, f32[8,1,128,256]{3,2,1,0:T(8,128)}, u32[]{:S(2)}) copy-start(f32[8,1,128,256]{3,2,1,0:T(8,128)} %state_ref.1) | copy-start | bytes 3145732
  34.5 12.3 %copy-start.6 = (bf16[256,256]{1,0:T(8,128)(2,1)S(1)}, bf16[256,256]{1,0:T(8,128)(2,1)}, u32[]{:S(2)}) copy-start(bf16[256,256]{1,0:T(8,128)(2,1)} %own_ref.1) | copy-start | bytes 393220
  46.8 13.2 %copy-start.1 = (bf16[256,704]{0,1:T(8,128)(2,1)S(1)}, bf16[256,704]{0,1:T(8,128)(2,1)}, u32[]{:S(2)}) copy-start(bf16[256,704]{0,1:T(8,128)(2,1)} %param.24) | copy-start | bytes 1081348
  47.0 13.0 %copy-start = (bf16[256,704]{0,1:T(8,128)(2,1)S(1)}, bf16[256,704]{0,1:T(8,128)(2,1)}, u32[]{:S(2)}) copy-start(bf16[256,704]{0,1:T(8,128)(2,1)} %param.23) | copy-start | bytes 1081348
  60.0 2.8 %collective-permute-start.1 = (bf16[128,128]{1,0:T(8,128)(2,1)S(1)}, bf16[128,128]{1,0:T(8,128)(2,1)S(1)}, u32[]{:S(2)}, u32[]{:S(2)}) collective-permute-start(bf16[128,128]{1,0:T(8,128)(2,1)S(1)} %shard_map.145.half_ref), channel_id=1, source_target_pairs={{0,1},{1,0},{2,3},{3,2},{4,5},{5,4},{6,7},{7,6},{8,9},{9,8},{10,11... | collective-permute-start | bytes 98312 | tf_op jit(solution)/shard_map/ppermute | solution.py:358
  74.8 10.3 %copy-start.3 = (bf16[704,256]{1,0:T(8,128)(2,1)S(1)}, bf16[704,256]{1,0:T(8,128)(2,1)}, u32[]{:S(2)}) copy-start(bf16[704,256]{1,0:T(8,128)(2,1)} %w_ref.1) | copy-start | bytes 1081348

commit v8 on v6

--- a/solution.py
+++ b/solution.py
@@ -207,7 +207,7 @@
         merged = jnp.concatenate(
             [merged_ref[i + which].astype(F32) for i in range(0, merged_ref.shape[0], 2)], axis=0
         )
-        weight = jnp.where(core == 0, w_ref[:, :half], w_ref[:, half:])
+        weight = w_ref[:, pl.ds(pl.multiple_of(core * half, half), half)]
         part = jnp.dot(merged.astype(BF16), weight, preferred_element_type=F32)
         total = part if total is None else total + part
     total = total.astype(BF16)

time: 98.8 us -> 98.7 us (level)
  no operation moved by 1% of the time
where the time goes in v8:
time: 98.7 us; the launch traced here: 98.4 us
  blocking collectives  86.9 us (88%)
  starting transfers between devices  6.42 us (7%)
  Pallas kernels  4.18 us (4%)
    all_to_all x7, blocking collectives, exchanged(): lax.all_to_all(blocks, axis, 0, 0, tiled=True, axis_index_groups=groups)  86.9 us
    pallas_call x11, Pallas kernels, local_call(): pl.pallas_call(kernel, out_shape=outs, in_specs=[pl.BlockSpec(memory_spac...  4.18 us
    ppermute x1, starting transfers between devices, on_device(): other_weight = lax.ppermute(output_weight, 'core', swap)  3.29 us
    ppermute x1, starting transfers between devices, on_device(): residual_other = lax.ppermute(residual_half, 'core', swap)  3.14 us
  transfers between devices with their start and end apart: 2, of which 0 were waited for; matrix products, arithmetic and copies ran while one was open for 0% of the time, Pallas kernels for 2%

profile of v8, /device:TPU:1, one launch (start us, length us, event | category | flops | bytes accessed | tf_op | source)
XLA Modules:
  0.0 98.4 jit_solution(18364880877277789140)
XLA Ops:
  0.6 3.3 %collective-permute-start = (bf16[256,256]{1,0:T(8,128)(2,1)}, bf16[256,256]{1,0:T(8,128)(2,1)S(1)}, u32[]{:S(2)}, u32[]{:S(2)}) collective-permute-start(bf16[256,256]{1,0:T(8,128)(2,1)} %own_ref.1), channel_id=1, source_target_pairs={{0,1},{1,0},{2,3},{3,2},{4,5},{5,4},{6,7},{7,6},{8,9},{9,8},{10,11... | collective-permute-start | bytes 393224 | tf_op jit(solution)/shard_map/ppermute | solution.py:324
  3.9 0.7 shard_map.140
  4.7 0.0 copy-start.4
  4.7 0.0 copy-start.5
  4.7 0.0 copy-start.7
  4.7 0.0 copy-start.8
  4.7 0.0 copy-start.2
  4.8 14.6 %all_to_all.35.x_ref = bf16[16,16,128]{2,1,0:T(8,128)(2,1)S(1)} all-to-all(bf16[16,16,128]{2,1,0:T(8,128)(2,1)S(1)} %shard_map.141), channel_id=1, replica_groups=mesh['kv'=16,'z'=8,'core'=2] {'z','core'}, dimensions={0} | all-to-all | bytes 131072 | tf_op jit(solution)/shard_map/all_to_all | solution.py:270
  19.3 0.0 collective-permute-done.other_ref
  19.3 0.0 copy-done.4
  19.3 0.0 copy-done.5
  19.3 0.0 copy-done.7
  19.4 0.0 copy-done.8
  19.4 0.3 shard_map.142
  19.6 14.3 %all_to_all.36.parts_ref = bf16[16,8,896]{2,1,0:T(8,128)(2,1)S(1)} all-to-all(bf16[16,8,896]{2,1,0:T(8,128)(2,1)S(1)} %get-tuple-element.21), channel_id=1, replica_groups={{0,128,240,224,80,32,48,176,96,208,160,64,144,112,16,192},{1,129,241,22..., dimensions={0} | all-to-all | bytes 458752 | tf_op jit(solution)/shard_map/all_to_all | solution.py:270
  33.9 0.0 copy-done.2
  33.9 0.6 shard_map.143
  34.5 0.0 copy-start.6
  34.5 12.3 %all_to_all.37.merged_ref = bf16[32,8,256]{2,1,0:T(8,128)(2,1)S(1)} all-to-all(bf16[32,8,256]{2,1,0:T(8,128)(2,1)S(1)} %get-tuple-element.24), channel_id=1, replica_groups=mesh['kv'=16,'z'=8,'core'=2] {'kv','core'}, dimensions={0} | all-to-all | bytes 262144 | tf_op jit(solution)/shard_map/all_to_all | solution.py:270
  46.8 0.0 copy-done.6
  46.8 0.0 copy-start.1
  46.8 0.2 shard_map.144
  47.0 0.0 copy-start
  47.0 10.7 %all_to_all.38.parts_ref = bf16[8,128,128]{2,1,0:T(8,128)(2,1)S(1)} all-to-all(bf16[8,128,128]{2,1,0:T(8,128)(2,1)S(1)} %shard_map.144), channel_id=1, replica_groups={{0,2,8,6,4,10,14,12},{1,3,9,7,5,11,15,13},{16,18,24,22,20,26,30,28},{17..., dimensions={0} | all-to-all | bytes 524288 | tf_op jit(solution)/shard_map/all_to_all | solution.py:270
  57.6 0.0 copy-done.1
  57.6 0.0 copy-done
  57.7 3.1 %collective-permute-start.1 = (bf16[128,128]{1,0:T(8,128)(2,1)S(1)}, bf16[128,128]{1,0:T(8,128)(2,1)S(1)}, u32[]{:S(2)}, u32[]{:S(2)}) collective-permute-start(bf16[128,128]{1,0:T(8,128)(2,1)S(1)} %shard_map.145.half_ref), channel_id=1, source_target_pairs={{0,1},{1,0},{2,3},{3,2},{4,5},{5,4},{6,7},{7,6},{8,9},{9,8},{10,11... | collective-permute-start | bytes 98312 | tf_op jit(solution)/shard_map/ppermute | solution.py:358
  60.8 1.0 shard_map.146
  61.8 0.0 collective-permute-done.1.other_ref
  61.8 0.4 shard_map.147
  62.2 11.7 %all_to_all.39.parts_ref = bf16[16,8,1536]{2,1,0:T(8,128)(2,1)S(1)} all-to-all(bf16[16,8,1536]{2,1,0:T(8,128)(2,1)S(1)} %get-tuple-element.31), channel_id=1, replica_groups={{0,128,240,224,80,32,48,176,96,208,160,64,144,112,16,192},{1,129,241,22..., dimensions={0} | all-to-all | bytes 786432 | tf_op jit(solution)/shard_map/all_to_all | solution.py:270
  73.9 0.0 copy-start.3
  73.9 0.1 shard_map.148
  74.0 10.2 %all_to_all.40.hidden_ref = bf16[16,8,704]{2,1,0:T(8,128)(2,1)S(1)} all-to-all(bf16[16,8,704]{2,1,0:T(8,128)(2,1)S(1)} %shard_map.148), channel_id=1, replica_groups={{0,128,240,224,80,32,48,176,96,208,160,64,144,112,16,192},{1,129,241,22..., dimensions={0} | all-to-all | bytes 360448 | tf_op jit(solution)/shard_map/all_to_all | solution.py:270
  84.2 0.0 copy-done.3
  84.2 0.3 shard_map.149
  84.5 13.2 %all_to_all.41.parts_ref = bf16[16,16,128]{2,1,0:T(8,128)(2,1)S(1)} all-to-all(bf16[16,16,128]{2,1,0:T(8,128)(2,1)S(1)} %shard_map.149), channel_id=1, replica_groups={{1,0,2,3,4,5,6,7,8,9,10,11,12,13,14,15},{17,16,18,19,20,21,22,23,24,25,..., dimensions={0} | all-to-all | bytes 131072 | tf_op jit(solution)/shard_map/all_to_all | solution.py:270
  97.7 0.6 shard_map.150
  (2 shorter events, 0.1 us)
Async XLA Ops:
  0.6 18.7 %collective-permute-start = (bf16[256,256]{1,0:T(8,128)(2,1)}, bf16[256,256]{1,0:T(8,128)(2,1)S(1)}, u32[]{:S(2)}, u32[]{:S(2)}) collective-permute-start(bf16[256,256]{1,0:T(8,128)(2,1)} %own_ref.1), channel_id=1, source_target_pairs={{0,1},{1,0},{2,3},{3,2},{4,5},{5,4},{6,7},{7,6},{8,9},{9,8},{10,11... | collective-permute-start | bytes 393224 | tf_op jit(solution)/shard_map/ppermute | solution.py:324
  4.7 14.7 %copy-start.4 = (bf16[256,256]{1,0:T(8,128)(2,1)S(1)}, bf16[256,256]{1,0:T(8,128)(2,1)}, u32[]{:S(2)}) copy-start(bf16[256,256]{1,0:T(8,128)(2,1)} %v_ref.1) | copy-start | bytes 393220
  4.7 14.7 %copy-start.5 = (bf16[256,256]{1,0:T(8,128)(2,1)S(1)}, bf16[256,256]{1,0:T(8,128)(2,1)}, u32[]{:S(2)}) copy-start(bf16[256,256]{1,0:T(8,128)(2,1)} %g_ref.1) | copy-start | bytes 393220
  4.7 14.7 %copy-start.7 = (bf16[256,128]{1,0:T(8,128)(2,1)S(1)}, bf16[256,128]{1,0:T(8,128)(2,1)}, u32[]{:S(2)}) copy-start(bf16[256,128]{1,0:T(8,128)(2,1)} %q_ref.1) | copy-start | bytes 196612
  4.7 14.6 %copy-start.8 = (bf16[256,128]{1,0:T(8,128)(2,1)S(1)}, bf16[256,128]{1,0:T(8,128)(2,1)}, u32[]{:S(2)}) copy-start(bf16[256,128]{1,0:T(8,128)(2,1)} %k_ref.1) | copy-start | bytes 196612
  4.7 29.2 %copy-start.2 = (f32[8,1,128,256]{3,2,1,0:T(8,128)S(1)}, f32[8,1,128,256]{3,2,1,0:T(8,128)}, u32[]{:S(2)}) copy-start(f32[8,1,128,256]{3,2,1,0:T(8,128)} %state_ref.1) | copy-start | bytes 3145732
  34.5 12.3 %copy-start.6 = (bf16[256,256]{1,0:T(8,128)(2,1)S(1)}, bf16[256,256]{1,0:T(8,128)(2,1)}, u32[]{:S(2)}) copy-start(bf16[256,256]{1,0:T(8,128)(2,1)} %own_ref.1) | copy-start | bytes 393220
  46.8 10.9 %copy-start.1 = (bf16[256,704]{0,1:T(8,128)(2,1)S(1)}, bf16[256,704]{0,1:T(8,128)(2,1)}, u32[]{:S(2)}) copy-start(bf16[256,704]{0,1:T(8,128)(2,1)} %param.24) | copy-start | bytes 1081348
  47.0 10.7 %copy-start = (bf16[256,704]{0,1:T(8,128)(2,1)S(1)}, bf16[256,704]{0,1:T(8,128)(2,1)}, u32[]{:S(2)}) copy-start(bf16[256,704]{0,1:T(8,128)(2,1)} %param.23) | copy-start | bytes 1081348
  57.7 4.1 %collective-permute-start.1 = (bf16[128,128]{1,0:T(8,128)(2,1)S(1)}, bf16[128,128]{1,0:T(8,128)(2,1)S(1)}, u32[]{:S(2)}, u32[]{:S(2)}) collective-permute-start(bf16[128,128]{1,0:T(8,128)(2,1)S(1)} %shard_map.145.half_ref), channel_id=1, source_target_pairs={{0,1},{1,0},{2,3},{3,2},{4,5},{5,4},{6,7},{7,6},{8,9},{9,8},{10,11... | collective-permute-start | bytes 98312 | tf_op jit(solution)/shard_map/ppermute | solution.py:358
  73.9 10.3 %copy-start.3 = (bf16[704,256]{1,0:T(8,128)(2,1)S(1)}, bf16[704,256]{1,0:T(8,128)(2,1)}, u32[]{:S(2)}) copy-start(bf16[704,256]{1,0:T(8,128)(2,1)} %w_ref.1) | copy-start | bytes 1081348
